TPU v7x, 32 devices: a whole 2x2x4 slice. The times are simulated.
32 devices in a mesh: sp: 4 (over z), fs: 4 (over y, x), tp: 2 (over core).
Axes of the slice: x: 2, y: 2, z: 4, core: 2. Of those that a mesh axis runs over, the one named last changes fastest.
Arguments:
- tokens: bfloat16 [6144, 2048], P(('fs', 'sp', 'tp')), parts along dimension 0, may hold values from -6 to 6
- norm_gain: float32 [2048], replicated, may hold values from 0.1 to 1.9
- w_input: bfloat16 [2048, 1024], P(None, 'tp'), may hold values from -0.125 to 0.125
- w_query: bfloat16 [2048, 1024], P(None, 'tp'), may hold values from -0.125 to 0.125
- w_key: bfloat16 [2048, 1024], P(None, 'tp'), may hold values from -0.125 to 0.125
- w_value: bfloat16 [2048, 1024], P(None, 'tp'), may hold values from -0.125 to 0.125
- query_gain: float32 [64], replicated, may hold values from 0.1 to 1.9
- key_gain: float32 [64], replicated, may hold values from 0.1 to 1.9
- key_bias: bfloat16 [6144, 16], P(('fs', 'sp'), 'tp'), parts along dimension 0, may hold values from -16 to 0
- eigen_real: float32 [64, 64], P('tp'), may hold values from -32 to 0
- eigen_imag: float32 [64, 64], P('tp'), may hold values from 0.31 to 201.0624
- log_step: float32 [64], P('tp'), may hold values from -6.91 to -2.3
- input_real: float32 [64, 64, 16], P('tp'), may hold values from -1 to 1
- input_imag: float32 [64, 64, 16], P('tp'), may hold values from -1 to 1
- read_real: float32 [64, 16, 64], P('tp'), may hold values from -0.75 to 0.75
- read_imag: float32 [64, 16, 64], P('tp'), may hold values from -0.75 to 0.75
- skip_gain: float32 [1024], P('tp'), may hold values from -6 to 6
- w_out_state: bfloat16 [1024, 2048], P('tp'), may hold values from -0.125 to 0.125
- w_out_attn: bfloat16 [1024, 2048], P('tp'), may hold values from -0.125 to 0.125
Outputs:
- layer_out: bfloat16 [6144, 2048], P(('fs', 'sp', 'tp')), parts along dimension 0
There are 4 independent parts, one for each index of `fs`. A program takes and returns all parts, laid end to end along the dimension named above; an argument that names none is the same for every part. Nothing has to cross between parts.
All inputs are finite; a program needn't handle non-finite values.
Results may differ from a plain program's by a relative error of at most 0.014.
Values may be sent and summed in bfloat16 or wider, within the bound.
A program may use at most 128 MiB of HBM per device.

v0:
```python
import functools

import jax
import jax.numpy as jnp
from jax import lax
from jax.experimental import pallas as pl
from jax.experimental.pallas import tpu as pltpu
from jax.sharding import PartitionSpec as P

GROUP = 16
STATE = 64
HEAD_DIM = 64


EPSILON = 1e-06
PRECISE = lax.Precision.HIGHEST


def from_behind(block, axis, distance):
    devices = range(lax.axis_size(axis))
    route = [(i - distance, i) for i in devices if i - distance in devices]
    return lax.ppermute(block, axis, route)


def carried_in(part, axis, combine, identity):
    place = lax.axis_index(axis)
    gathered = jax.tree.map(lambda a: lax.all_gather(a, axis), part)
    state = jax.tree.map(lambda a, e: jnp.zeros_like(a) + jnp.asarray(e, a.dtype), part, identity)

    def one(lap, state):
        return combine(
            state, jax.tree.map(lambda a: lax.dynamic_index_in_dim(a, lap, 0, False), gathered)
        )

    return lax.fori_loop(0, place, one, state)


def combine_states(earlier, later):
    leading_real_factor, first_ai, first_br, first_bi = earlier
    second_ar, second_ai, second_br, second_bi = later
    prod_r = second_ar * leading_real_factor - second_ai * first_ai
    prod_i = second_ar * first_ai + second_ai * leading_real_factor
    state_r = second_ar * first_br - second_ai * first_bi + second_br
    state_i = second_ar * first_bi + second_ai * first_br + second_bi
    return (prod_r, prod_i, state_r, state_i)


def discretize(eigen_real, eigen_imag, log_step, input_real, input_imag):
    step_size = jnp.exp(log_step)[:, None]
    rotation = eigen_imag * step_size
    shrink = jnp.expm1(eigen_real * step_size)
    cosine = jnp.cos(rotation)
    sine_part = jnp.sin(rotation)
    decay_r = (1.0 + shrink) * cosine
    decay_i = (1.0 + shrink) * sine_part
    minus_r = shrink * cosine - 2.0 * jnp.square(jnp.sin(0.5 * rotation))
    modulus = jnp.square(eigen_real) + jnp.square(eigen_imag)
    factor_r = (minus_r * eigen_real + decay_i * eigen_imag) / modulus
    factor_i = (decay_i * eigen_real - minus_r * eigen_imag) / modulus
    drive_r = factor_r[..., None] * input_real - factor_i[..., None] * input_imag
    drive_i = factor_r[..., None] * input_imag + factor_i[..., None] * input_real
    return (decay_r, decay_i, drive_r, drive_i)


def head_scale(flat_rows, head_gain, head_count):
    row_count = flat_rows.shape[0]
    shaped = flat_rows.astype(jnp.float32).reshape(row_count, head_count, HEAD_DIM)
    scaled = shaped * lax.rsqrt(jnp.mean(jnp.square(shaped), axis=-1, keepdims=True) + EPSILON)
    return (scaled * head_gain).astype(jnp.bfloat16)


def block_terms(queries, key_rows, value_rows, bias_rows, q_first, k_first):
    head_count = queries.shape[1]
    key_heads = key_rows.reshape(key_rows.shape[0], head_count, HEAD_DIM)
    value_heads = value_rows.reshape(value_rows.shape[0], head_count, HEAD_DIM)
    scores = jnp.einsum("qhd,khd->hqk", queries, key_heads, preferred_element_type=jnp.float32)
    scores = scores * HEAD_DIM ** (-0.5) + jnp.transpose(bias_rows.astype(jnp.float32))[:, None, :]
    query_place = q_first + lax.iota(jnp.int32, queries.shape[0])
    key_place = k_first + lax.iota(jnp.int32, key_rows.shape[0])
    causal = (key_place[None, :] < query_place[:, None])[None]
    log_keep = jnp.where(causal, jax.nn.log_sigmoid(-scores), 0.0)
    trailing_sum = lax.cumsum(log_keep, axis=2, reverse=True) - log_keep
    weights = jnp.where(causal, jnp.exp(jax.nn.log_sigmoid(scores) + trailing_sum), 0.0).astype(
        jnp.bfloat16
    )
    block_out = jnp.einsum("hqk,khd->qhd", weights, value_heads, preferred_element_type=jnp.float32)
    return (block_out.reshape(queries.shape[0], head_count * HEAD_DIM), jnp.sum(log_keep, axis=2))


def guarded_terms(queries, key_rows, value_rows, bias_rows, q_first, k_first):
    live = jnp.logical_and(k_first >= 0, k_first <= q_first)

    def compute_block():
        return block_terms(queries, key_rows, value_rows, bias_rows, q_first, k_first)

    def empty_block():
        return (
            jnp.zeros((queries.shape[0], queries.shape[1] * HEAD_DIM), jnp.float32),
            jnp.zeros((queries.shape[1], queries.shape[0]), jnp.float32),
        )

    return lax.cond(live, compute_block, empty_block)


def merge_blocks(block_parts, totals):
    blocks, row_count, row_width = block_parts.shape
    head_count = totals.shape[1]
    later_sum = jnp.flip(jnp.cumsum(jnp.flip(totals, 0), axis=0), 0) - totals
    factors = jnp.exp(jnp.transpose(later_sum, (0, 2, 1)))[..., None]

    def add_block(block_idx, accumulated):
        part = lax.dynamic_index_in_dim(block_parts, block_idx, 0, keepdims=False)
        factor = lax.dynamic_index_in_dim(factors, block_idx, 0, keepdims=False)
        return accumulated + part.reshape(row_count, head_count, HEAD_DIM) * factor

    accumulated = lax.fori_loop(
        0, blocks, add_block, jnp.zeros((row_count, head_count, HEAD_DIM), jnp.float32)
    )
    normed = accumulated * lax.rsqrt(
        jnp.mean(jnp.square(accumulated), axis=-1, keepdims=True) + EPSILON
    )
    return normed.reshape(row_count, row_width).astype(jnp.bfloat16)


def attend(queries, key_rows, value_rows, bias_rows):
    row_count = queries.shape[0]
    head_count = queries.shape[1]
    row_width = key_rows.shape[1]
    my_first = lax.axis_index("sp") * row_count
    levels = (lax.axis_size("sp") - 1).bit_length()
    slot_count = 2**levels
    own_out, own_totals = block_terms(queries, key_rows, value_rows, bias_rows, my_first, my_first)
    block_parts = lax.dynamic_update_slice_in_dim(
        jnp.zeros((slot_count, row_count, row_width), jnp.float32), own_out[None], 0, 0
    )
    totals = lax.dynamic_update_slice_in_dim(
        jnp.zeros((slot_count, head_count, row_count), jnp.float32), own_totals[None], 0, 0
    )
    held_keys = (key_rows, value_rows, bias_rows)
    for level_idx in range(levels):
        distance_base = 2**level_idx
        arrived = from_behind((held_keys[0], held_keys[1], held_keys[2]), "sp", distance_base)

        def one_block(inner_idx, current, arrived=arrived, distance_base=distance_base):
            offset = inner_idx * row_count
            distance = distance_base + inner_idx
            k_first = my_first - distance * row_count
            block_out, block_totals = guarded_terms(
                queries,
                lax.dynamic_slice_in_dim(arrived[0], offset, row_count, 0),
                lax.dynamic_slice_in_dim(arrived[1], offset, row_count, 0),
                lax.dynamic_slice_in_dim(arrived[2], offset, row_count, 0),
                my_first,
                k_first,
            )
            return (
                lax.dynamic_update_slice_in_dim(current[0], block_out[None], distance, 0),
                lax.dynamic_update_slice_in_dim(current[1], block_totals[None], distance, 0),
            )

        block_parts, totals = lax.fori_loop(0, distance_base, one_block, (block_parts, totals))
        if level_idx + 1 < levels:
            held_keys = (
                jnp.concatenate([held_keys[0], arrived[0]], axis=0),
                jnp.concatenate([held_keys[1], arrived[1]], axis=0),
                jnp.concatenate([held_keys[2], arrived[2]], axis=0),
            )
    return merge_blocks(jnp.flip(block_parts, 0), jnp.flip(totals, 0))


def state_branch(
    inputs,
    eigen_real,
    eigen_imag,
    log_step,
    input_real,
    input_imag,
    read_real,
    read_imag,
    skip_gain,
):
    decay_r, decay_i, drive_r, drive_i = discretize(
        eigen_real, eigen_imag, log_step, input_real, input_imag
    )
    row_count = inputs.shape[0]
    groups = eigen_real.shape[0]
    inputs_wide = inputs.astype(jnp.float32)
    grouped = inputs_wide.reshape(row_count, groups, GROUP)
    push_r = jnp.einsum("lgh,gph->lgp", grouped, drive_r, precision=PRECISE).reshape(
        row_count, groups * STATE
    )
    push_i = jnp.einsum("lgh,gph->lgp", grouped, drive_i, precision=PRECISE).reshape(
        row_count, groups * STATE
    )
    steps_r = jnp.broadcast_to(decay_r.reshape(1, groups * STATE), push_r.shape)
    steps_i = jnp.broadcast_to(decay_i.reshape(1, groups * STATE), push_i.shape)
    running = lax.associative_scan(combine_states, (steps_r, steps_i, push_r, push_i), axis=0)
    block_ends = (
        running[0][row_count - 1],
        running[1][row_count - 1],
        running[2][row_count - 1],
        running[3][row_count - 1],
    )
    identity = (
        jnp.ones((groups * STATE,), jnp.float32),
        jnp.zeros((groups * STATE,), jnp.float32),
        jnp.zeros((groups * STATE,), jnp.float32),
        jnp.zeros((groups * STATE,), jnp.float32),
    )
    before = carried_in(block_ends, "sp", combine_states, identity)
    state_r = running[2] + running[0] * before[2][None, :] - running[1] * before[3][None, :]
    state_i = running[3] + running[0] * before[3][None, :] + running[1] * before[2][None, :]
    readout = jnp.einsum(
        "lgp,ghp->lgh", state_r.reshape(row_count, groups, STATE), read_real, precision=PRECISE
    )
    readout = readout - jnp.einsum(
        "lgp,ghp->lgh", state_i.reshape(row_count, groups, STATE), read_imag, precision=PRECISE
    )
    mixed = readout.reshape(row_count, groups * GROUP) + skip_gain * inputs_wide
    return jax.nn.gelu(mixed).astype(jnp.bfloat16)


def plain_device(
    tokens,
    norm_gain,
    w_input,
    w_query,
    w_key,
    w_value,
    query_gain,
    key_gain,
    key_bias,
    eigen_real,
    eigen_imag,
    log_step,
    input_real,
    input_imag,
    read_real,
    read_imag,
    skip_gain,
    w_out_state,
    w_out_attn,
):
    token_rows = tokens.astype(jnp.float32)
    scale_rows = lax.rsqrt(jnp.mean(jnp.square(token_rows), axis=-1, keepdims=True) + EPSILON)
    normed = (token_rows * scale_rows * norm_gain).astype(jnp.bfloat16)
    w_joined = jnp.concatenate([w_input, w_query, w_key, w_value], axis=1)
    projected = jnp.dot(
        lax.all_gather(normed, "tp", axis=0, tiled=True),
        w_joined,
        preferred_element_type=jnp.float32,
    ).astype(jnp.bfloat16)
    state_width = w_input.shape[1]
    attn_width = w_query.shape[1]
    head_count = attn_width // HEAD_DIM
    inputs = projected[:, :state_width]
    query_rows = projected[:, state_width : state_width + attn_width]
    key_rows = projected[:, state_width + attn_width : state_width + 2 * attn_width]
    value_rows = projected[:, state_width + 2 * attn_width :]
    queries = head_scale(query_rows, query_gain, head_count)
    key_normed = head_scale(key_rows, key_gain, head_count).reshape(key_rows.shape[0], attn_width)
    attn_out = attend(queries, key_normed, value_rows, key_bias)
    state_out = state_branch(
        inputs,
        eigen_real,
        eigen_imag,
        log_step,
        input_real,
        input_imag,
        read_real,
        read_imag,
        skip_gain,
    )
    summed_part = jnp.dot(state_out, w_out_state, preferred_element_type=jnp.float32)
    return lax.psum_scatter(
        (summed_part + jnp.dot(attn_out, w_out_attn, preferred_element_type=jnp.float32)).astype(
            jnp.bfloat16
        ),
        "tp",
        scatter_dimension=0,
        tiled=True,
    )


LANES = 128
NT = (((1,), (1,)), ((), ()))


def dot_nt(a, b):
    return lax.dot_general(a, b, NT, preferred_element_type=jnp.float32)


def dot_nn(a, b):
    return jnp.dot(a, b, preferred_element_type=jnp.float32)


def by_head(low, high, shape):
    return jnp.where(lax.broadcasted_iota(jnp.int32, shape, 1) < HEAD_DIM, low, high)


def head_rms(rows):
    square = rows * rows
    low = jnp.sum(by_head(square, 0.0, rows.shape), axis=-1, keepdims=True)
    high = jnp.sum(by_head(0.0, square, rows.shape), axis=-1, keepdims=True)
    mean = by_head(low, high, rows.shape) * (1.0 / HEAD_DIM)
    return rows * lax.rsqrt(mean + EPSILON)


def complex_power(real, imag, exponent):
    out_r, out_i = None, None
    while exponent:
        if exponent & 1:
            if out_r is None:
                out_r, out_i = real, imag
            else:
                out_r, out_i = out_r * real - out_i * imag, out_r * imag + out_i * real
        exponent >>= 1
        if exponent:
            real, imag = real * real - imag * imag, 2.0 * real * imag
    return out_r, out_i


def mixer_kernel(
    ranks,
    tokens_ref,
    norm_gain_ref,
    w_input_ref,
    w_query_ref,
    w_key_ref,
    w_value_ref,
    w_state_ref,
    w_attn_ref,
    q_gain_ref,
    k_gain_ref,
    bias_ref,
    decay_r_ref,
    decay_i_ref,
    factor_r_ref,
    factor_i_ref,
    input_r_ref,
    input_i_ref,
    read_r_ref,
    read_i_ref,
    skip_ref,
    out_ref,
    normed,
    decay_ref,
    state_part,
    w_held,
    w_out,
    act_ref,
    u_ref,
    v_ref,
    q_norm,
    k_norm,
    bias_stage,
    out_part,
    out_arrived,
    w_sem,
    row_sem,
    part_send,
    part_recv,
    q_land,
    k_land,
    v_land,
    bias_land,
    push_r,
    push_i,
    up_ref,
    seg_r,
    seg_i,
    ends_land,
    q_two,
    acc_ref,
    run_ref,
    out_stage,
    out_land,
    local_sem,
    send_sem,
    recv_sem,
    end_send,
    end_recv,
    back_send,
    back_recv,
):
    rows, width = u_ref.shape
    states = decay_ref.shape[1]
    chunks = rows // LANES
    seg_len = rows // 8
    own_count, features = tokens_ref.shape
    core = lax.axis_index("tp")
    own_rows = pl.ds(pl.multiple_of(core * own_count, own_count), own_count)
    mate_rows = pl.ds(pl.multiple_of((1 - core) * own_count, own_count), own_count)
    mate = {"device_id": {"tp": 1 - core}, "device_id_type": pl.DeviceIdType.MESH}
    halves = width // 256
    span = states // halves
    me = lax.axis_index("sp")
    others = range(1, ranks)

    def at_rank(step):
        return lax.rem(me + step, ranks)

    barrier = pltpu.get_barrier_semaphore()
    for step in others:
        pl.semaphore_signal(
            barrier, inc=1, device_id={"sp": at_rank(step)}, device_id_type=pl.DeviceIdType.MESH
        )

    pl.semaphore_signal(barrier, inc=1, **mate)
    weights = []
    for slot, ref in enumerate((w_key_ref, w_value_ref, w_query_ref, w_input_ref)):
        weights.append(pltpu.make_async_copy(ref, w_held.at[slot], w_sem.at[slot]))
    for slot, ref in enumerate((w_state_ref, w_attn_ref)):
        target = w_out.at[slot * width : (slot + 1) * width, :]
        weights.append(pltpu.make_async_copy(ref, target, w_sem.at[4 + slot]))
    for copy in weights:
        copy.start()

    token_rows = tokens_ref[...].astype(jnp.float32)
    mean = jnp.sum(token_rows * token_rows, axis=-1, keepdims=True) * (1.0 / features)
    scaled = token_rows * lax.rsqrt(mean + EPSILON) * norm_gain_ref[...]
    normed[own_rows, :] = scaled.astype(jnp.bfloat16)
    bias = bias_ref[...].astype(jnp.float32)
    for rank in range(ranks):
        for chunk in range(chunks):
            bias_stage[rank, chunk] = bias[
                2 * rank : 2 * rank + 2, chunk * LANES : (chunk + 1) * LANES
            ]
    q_gain, k_gain = (
        jnp.concatenate([ref[...], ref[...]], axis=1) for ref in (q_gain_ref, k_gain_ref)
    )
    groups = decay_r_ref.shape[0]
    for row, ref in enumerate((decay_r_ref, decay_i_ref)):
        decay_ref[row : row + 1, :] = jnp.concatenate(
            [ref[group : group + 1, :] for group in range(groups)], axis=1
        )

    pl.semaphore_wait(barrier, ranks)
    row_copy = pltpu.make_async_remote_copy(
        src_ref=normed.at[own_rows, :],
        dst_ref=normed.at[own_rows, :],
        send_sem=row_sem.at[0],
        recv_sem=row_sem.at[1],
        **mate,
    )
    row_copy.start()

    def project(slot, at):
        flat = dot_nn(normed[at, :], w_held[slot]).astype(jnp.bfloat16)
        if slot == 1:
            v_ref[at, :] = flat
        elif slot == 3:
            u_ref[at, :] = flat
        else:
            gain, target, scale = (
                (k_gain, k_norm, 1.0) if slot == 0 else (q_gain, q_norm, HEAD_DIM**-0.5)
            )
            for tile in range(width // LANES):
                cols = slice(tile * LANES, (tile + 1) * LANES)
                part = head_rms(flat[:, cols].astype(jnp.float32)) * gain
                target[at, cols] = part.astype(jnp.bfloat16) * jnp.bfloat16(scale)

    for slot in range(4):
        weights[slot].wait()
        project(slot, own_rows)
    row_copy.wait_recv()

    my_rows = pl.ds(pl.multiple_of(me * rows, rows), rows)

    def piece(kind, rank):
        cols = pl.ds(pl.multiple_of(rank * LANES, LANES), LANES)
        if kind == 3:
            return bias_stage.at[rank], bias_land.at[pl.ds(me * chunks, chunks)]
        source, target = ((k_norm, k_land), (v_ref, v_land), (q_norm, q_land))[kind]
        return source.at[:, cols], target.at[my_rows, :]

    sends = []
    local = []

    def redistribute(kind):
        for step in others:
            source, target = piece(kind, at_rank(step))
            copy = pltpu.make_async_remote_copy(
                src_ref=source,
                dst_ref=target,
                send_sem=send_sem.at[step, kind],
                recv_sem=recv_sem.at[step, kind],
                device_id={"sp": at_rank(step)},
                device_id_type=pl.DeviceIdType.MESH,
            )
            copy.start()
            sends.append(copy)
        source, target = piece(kind, me)
        copy = pltpu.make_async_copy(source, target, local_sem.at[kind])
        copy.start()
        local.append(copy)

    redistribute(3)
    project(0, mate_rows)
    redistribute(0)
    project(3, mate_rows)

    def place(axis):
        index = lax.broadcasted_iota(jnp.int32, (rows, rows), axis)
        other = lax.broadcasted_iota(jnp.int32, (rows, rows), 1 - axis)
        return jnp.where(other == (index & 7) * seg_len + (index >> 3), 1.0, 0.0).astype(
            jnp.bfloat16
        )

    up_ref[...] = dot_nn(place(0), u_ref[...]).astype(jnp.bfloat16)

    spread_state = lax.broadcasted_iota(jnp.int32, (STATE, span), 0) == (
        lax.broadcasted_iota(jnp.int32, (STATE, span), 1) & (STATE - 1)
    )
    spread_state = jnp.where(spread_state, 1.0, 0.0).astype(jnp.bfloat16)

    def by_channel(ref):
        wide = jnp.broadcast_to(ref[...][:, None, :], (groups, GROUP, STATE))
        return wide.reshape(groups * GROUP, STATE)

    factor_r = by_channel(factor_r_ref)
    factor_i = by_channel(factor_i_ref)
    drive_r = factor_r * input_r_ref[...] - factor_i * input_i_ref[...]
    drive_i = factor_r * input_i_ref[...] + factor_i * input_r_ref[...]

    def block_diagonal(values, half):
        row_group = lax.broadcasted_iota(jnp.int32, (256, span), 0) // GROUP
        col_group = lax.broadcasted_iota(jnp.int32, (256, span), 1) // STATE
        wide = dot_nn(
            values[half * 256 : (half + 1) * 256, :].astype(jnp.bfloat16), spread_state
        )
        return jnp.where(row_group == col_group, wide, 0.0).astype(jnp.bfloat16)

    for half in range(halves):
        cols = slice(half * span, (half + 1) * span)
        part = up_ref[:, half * 256 : (half + 1) * 256]
        push_r[:, cols] = dot_nn(part, block_diagonal(drive_r, half))
        push_i[:, cols] = dot_nn(part, block_diagonal(drive_i, half))

    block = 512

    def scan(keep_states):
        for first in range(0, states, block):
            cols = slice(first, first + block)
            step_r = jnp.broadcast_to(decay_ref[0:1, cols], (8, block))
            step_i = jnp.broadcast_to(decay_ref[1:2, cols], (8, block))

            def one(index, state, cols=cols, step_r=step_r, step_i=step_i):
                state_r, state_i = state
                at = pl.ds(pl.multiple_of(index * 8, 8), 8)
                next_r = step_r * state_r - step_i * state_i + push_r[at, cols]
                next_i = step_r * state_i + step_i * state_r + push_i[at, cols]
                if keep_states:
                    push_r[at, cols] = next_r
                    push_i[at, cols] = next_i
                return (next_r, next_i)

            if keep_states:
                start = (seg_r[:, cols], seg_i[:, cols])
            else:
                start = (jnp.zeros((8, block), jnp.float32),) * 2
            state_r, state_i = lax.fori_loop(0, seg_len, one, start, unroll=4)
            if not keep_states:
                seg_r[:, cols] = state_r
                seg_i[:, cols] = state_i

    scan(False)
    seg_step_r, seg_step_i = complex_power(decay_ref[0:1, :], decay_ref[1:2, :], seg_len)
    end_r = jnp.zeros((1, states), jnp.float32)
    end_i = jnp.zeros((1, states), jnp.float32)
    for seg in range(8):
        end_r, end_i = (
            seg_step_r * end_r - seg_step_i * end_i + seg_r[seg : seg + 1, :],
            seg_step_r * end_i + seg_step_i * end_r + seg_i[seg : seg + 1, :],
        )
    ends_land[me, 0:1, :] = end_r
    ends_land[me, 1:2, :] = end_i
    end_copies = []
    for step in others:
        copy = pltpu.make_async_remote_copy(
            src_ref=ends_land.at[me],
            dst_ref=ends_land.at[me],
            send_sem=end_send.at[step],
            recv_sem=end_recv.at[step],
            device_id={"sp": at_rank(step)},
            device_id_type=pl.DeviceIdType.MESH,
        )
        copy.start()
        end_copies.append(copy)

    project(1, mate_rows)
    redistribute(1)
    project(2, mate_rows)
    redistribute(2)

    for copy in end_copies:
        copy.wait_recv()
    block_r, block_i = complex_power(decay_ref[0:1, :], decay_ref[1:2, :], rows)
    carry_r = jnp.zeros((1, states), jnp.float32)
    carry_i = jnp.zeros((1, states), jnp.float32)
    for rank in range(ranks - 1):
        next_r = block_r * carry_r - block_i * carry_i + ends_land[rank, 0:1, :]
        next_i = block_r * carry_i + block_i * carry_r + ends_land[rank, 1:2, :]
        carry_r = jnp.where(rank < me, next_r, carry_r)
        carry_i = jnp.where(rank < me, next_i, carry_i)
    for seg in range(8):
        own_r = seg_r[seg : seg + 1, :]
        own_i = seg_i[seg : seg + 1, :]
        seg_r[seg : seg + 1, :] = carry_r
        seg_i[seg : seg + 1, :] = carry_i
        carry_r, carry_i = (
            seg_step_r * carry_r - seg_step_i * carry_i + own_r,
            seg_step_r * carry_i + seg_step_i * carry_r + own_i,
        )
    scan(True)

    back = place(1)
    for half in range(halves):
        cols = slice(half * 256, (half + 1) * 256)
        mixed = skip_ref[:, cols] * up_ref[:, cols].astype(jnp.float32)
        for read, held in ((read_r_ref[...], push_r), (-read_i_ref[...], push_i)):
            mixed = mixed + dot_nt(
                held[:, half * span : (half + 1) * span].astype(jnp.bfloat16),
                block_diagonal(read, half),
            )
        act_ref[:, cols] = dot_nn(back, jax.nn.gelu(mixed).astype(jnp.bfloat16)).astype(
            jnp.bfloat16
        )

    for copy in weights[4:]:
        copy.wait()
    pieces = out_part.shape[0]
    piece_width = out_part.shape[2]

    def piece_cols(index):
        return pl.ds(pl.multiple_of(index * piece_width, piece_width), piece_width)

    def state_piece(index, carry):
        state_part[:, piece_cols(index)] = dot_nn(
            act_ref[:, :width], w_out[:width, piece_cols(index)]
        )
        return carry

    lax.fori_loop(0, pieces, state_piece, 0)

    for copy in local:
        copy.wait()
    for copy in sends:
        copy.wait_recv()

    tail = lax.broadcasted_iota(jnp.int32, (LANES, 2 * LANES), 0)
    col = lax.broadcasted_iota(jnp.int32, (LANES, 2 * LANES), 1)
    tail = jnp.where(jnp.logical_or(tail >= col, col >= LANES), 1.0, 0.0).astype(jnp.bfloat16)
    lane = lax.broadcasted_iota(jnp.int32, (1, LANES), 1)
    low_mask = jnp.where(lane < HEAD_DIM, 1.0, 0.0).astype(jnp.bfloat16)
    high_mask = jnp.where(lane < HEAD_DIM, 0.0, 1.0).astype(jnp.bfloat16)

    def chunk_step(chunk, first, diagonal):
        count = rows - first
        at = pl.ds(pl.multiple_of(chunk * LANES, LANES), LANES)
        keys = k_land[at, :]
        values = v_land[at, :]
        values = jnp.concatenate([values * low_mask, values * high_mask], axis=0)
        probs = []
        for head in range(2):
            span_rows = slice(head * rows + first, (head + 1) * rows)
            z = dot_nt(q_two[span_rows, :], keys) + bias_land[chunk, head : head + 1, :]
            keep = jnp.minimum(-z, 0.0) - jnp.log(1.0 + jnp.exp(-jnp.abs(z)))
            if diagonal:
                causal = lax.broadcasted_iota(
                    jnp.int32, (count, LANES), 1
                ) < lax.broadcasted_iota(jnp.int32, (count, LANES), 0)
                keep = jnp.where(causal, keep, 0.0)
            sums = dot_nn(keep.astype(jnp.bfloat16), tail)
            running = run_ref[span_rows, :]
            weight = jnp.exp(z + sums[:, :LANES] + running)
            if diagonal:
                weight = jnp.where(causal, weight, 0.0)
            run_ref[span_rows, :] = running + sums[:, LANES:]
            probs.append(weight.astype(jnp.bfloat16))
        acc_ref[first:, :] += dot_nn(jnp.concatenate(probs, axis=1), values)

    def back_copy(step):
        rank = at_rank(step)
        return pltpu.make_async_remote_copy(
            src_ref=out_stage.at[rank],
            dst_ref=out_land.at[me],
            send_sem=back_send.at[step],
            recv_sem=back_recv.at[step],
            device_id={"sp": rank},
            device_id_type=pl.DeviceIdType.MESH,
        )

    def query_block(step, carry):
        rank = at_rank(step)
        queries = q_land[pl.ds(pl.multiple_of(rank * rows, rows), rows), :]
        q_two[:rows, :] = queries * low_mask
        q_two[rows:, :] = queries * high_mask
        acc_ref[...] = jnp.zeros_like(acc_ref)
        run_ref[...] = jnp.zeros_like(run_ref)
        for part in reversed(range(chunks)):
            chunk_step(rank * chunks + part, part * LANES, True)

        def earlier(index, inner):
            for part in reversed(range(chunks)):
                chunk_step((rank - 1 - index) * chunks + part, 0, False)
            return inner

        lax.fori_loop(0, rank, earlier, 0)
        out_stage[rank] = head_rms(acc_ref[...]).astype(jnp.bfloat16)

        @pl.when(step < ranks)
        def _():
            back_copy(step).start()

        return carry

    lax.fori_loop(1, ranks + 1, query_block, 0)

    out_land[me] = out_stage[me]
    for step in others:
        back_copy(step).wait_recv()
    for rank in range(ranks):
        act_ref[:, width + rank * LANES : width + (rank + 1) * LANES] = out_land[rank]
    def part_copy(index):
        return pltpu.make_async_remote_copy(
            src_ref=out_part.at[index],
            dst_ref=out_arrived.at[index],
            send_sem=part_send.at[index],
            recv_sem=part_recv.at[index],
            **mate,
        )

    def piece_of(index, at):
        cols = piece_cols(index)
        return cols, state_part[at, cols] + dot_nn(act_ref[at, width:], w_out[width:, cols])

    def send_piece(index, carry):
        out_part[index] = piece_of(index, mate_rows)[1].astype(jnp.bfloat16)
        part_copy(index).start()
        return carry

    def own_piece(index, carry):
        cols, own = piece_of(index, own_rows)
        part_copy(index).wait_recv()
        out_ref[:, cols] = (own + out_arrived[index].astype(jnp.float32)).astype(jnp.bfloat16)
        return carry

    lax.fori_loop(0, pieces, send_piece, 0)
    lax.fori_loop(0, pieces, own_piece, 0)

    row_copy.wait_send()
    for index in range(pieces):
        part_copy(index).wait_send()
    for copy in sends + end_copies:
        copy.wait_send()
    for step in others:
        back_copy(step).wait_send()


def layer(ranks, tokens, norm_gain, weights, gains, key_bias, plan):
    count, features = tokens.shape
    width = weights[0].shape[1]
    rows = key_bias.shape[0]
    states = plan[0].size
    chunks = rows // LANES
    pieces = features // 512
    bias = key_bias.T
    gains = [gain[None, :] for gain in gains]
    dma = pltpu.SemaphoreType.DMA
    vmem = pl.BlockSpec(memory_space=pltpu.VMEM)
    hbm = pl.BlockSpec(memory_space=pl.ANY)
    half, full = jnp.bfloat16, jnp.float32
    return pl.pallas_call(
        functools.partial(mixer_kernel, ranks),
        out_shape=jax.ShapeDtypeStruct((count, features), jnp.bfloat16),
        in_specs=[vmem] * 2 + [hbm] * 6 + [vmem] * (3 + len(plan)),
        out_specs=vmem,
        scratch_shapes=[
            pltpu.VMEM((rows, features), half),
            pltpu.VMEM((2, states), full),
            pltpu.VMEM((rows, features), full),
            pltpu.VMEM((4, features, width), half),
            pltpu.VMEM((2 * width, features), half),
            pltpu.VMEM((rows, 2 * width), half),
            pltpu.VMEM((rows, width), half),
            pltpu.VMEM((rows, width), half),
            pltpu.VMEM((rows, width), half),
            pltpu.VMEM((rows, width), half),
            pltpu.VMEM((ranks, chunks, 2, LANES), full),
            pltpu.VMEM((pieces, count, 512), half),
            pltpu.VMEM((pieces, count, 512), half),
            dma((6,)),
            dma((2,)),
            dma((pieces,)),
            dma((pieces,)),
            pltpu.VMEM((ranks * rows, LANES), half),
            pltpu.VMEM((ranks * rows, LANES), half),
            pltpu.VMEM((ranks * rows, LANES), half),
            pltpu.VMEM((ranks * chunks, 2, LANES), full),
            pltpu.VMEM((rows, states), full),
            pltpu.VMEM((rows, states), full),
            pltpu.VMEM((rows, width), half),
            pltpu.VMEM((8, states), full),
            pltpu.VMEM((8, states), full),
            pltpu.VMEM((ranks, 2, states), full),
            pltpu.VMEM((2 * rows, LANES), half),
            pltpu.VMEM((rows, LANES), full),
            pltpu.VMEM((2 * rows, LANES), full),
            pltpu.VMEM((ranks, rows, LANES), half),
            pltpu.VMEM((ranks, rows, LANES), half),
            dma((4,)),
            dma((ranks, 4)),
            dma((ranks, 4)),
            dma((ranks,)),
            dma((ranks,)),
            dma((ranks + 1,)),
            dma((ranks + 1,)),
        ],
        compiler_params=pltpu.CompilerParams(
            collective_id=0, has_side_effects=True, vmem_limit_bytes=58 * 2**20
        ),
        name="layer",
    )(tokens, norm_gain[None, :], *weights, *gains, bias, *plan)


def on_device(
    tokens,
    norm_gain,
    w_input,
    w_query,
    w_key,
    w_value,
    query_gain,
    key_gain,
    key_bias,
    eigen_real,
    eigen_imag,
    log_step,
    input_real,
    input_imag,
    read_real,
    read_imag,
    skip_gain,
    w_out_state,
    w_out_attn,
):
    ranks = lax.axis_size("sp")
    width = w_query.shape[1]
    rows = key_bias.shape[0]
    fits = (
        ranks > 1
        and width == ranks * LANES
        and w_input.shape[1] == width
        and width % 256 == 0
        and rows % LANES == 0
        and lax.axis_size("tp") == 2
        and tokens.shape[1] % 512 == 0
    )
    if not fits:
        return plain_device(
            tokens,
            norm_gain,
            w_input,
            w_query,
            w_key,
            w_value,
            query_gain,
            key_gain,
            key_bias,
            eigen_real,
            eigen_imag,
            log_step,
            input_real,
            input_imag,
            read_real,
            read_imag,
            skip_gain,
            w_out_state,
            w_out_attn,
        )
    ones = jnp.ones_like(eigen_real)[..., None]
    decay_r, decay_i, factor_r, factor_i = discretize(
        eigen_real, eigen_imag, log_step, ones, jnp.zeros_like(ones)
    )
    plan = (
        decay_r,
        decay_i,
        factor_r[..., 0],
        factor_i[..., 0],
        jnp.transpose(input_real, (0, 2, 1)).reshape(-1, STATE),
        jnp.transpose(input_imag, (0, 2, 1)).reshape(-1, STATE),
        read_real.reshape(-1, STATE),
        read_imag.reshape(-1, STATE),
        skip_gain[None, :],
    )
    weights = (w_input, w_query, w_key, w_value, w_out_state, w_out_attn)
    return layer(ranks, tokens, norm_gain, weights, (query_gain, key_gain), key_bias, plan)


def solution(mesh):
    placed = (
        P(("fs", "sp", "tp"), None),
        P(),
        P(None, "tp"),
        P(None, "tp"),
        P(None, "tp"),
        P(None, "tp"),
        P(),
        P(),
        P(("fs", "sp"), "tp"),
        P("tp", None),
        P("tp", None),
        P("tp"),
        P("tp", None, None),
        P("tp", None, None),
        P("tp", None, None),
        P("tp", None, None),
        P("tp"),
        P("tp", None),
        P("tp", None),
    )
    return jax.shard_map(
        on_device,
        mesh=mesh,
        in_specs=placed,
        out_specs=P(("fs", "sp", "tp"), None),
        check_vma=False,
    )
```

profile of v0, /device:TPU:0, one launch (start us, length us, event | category | flops | bytes accessed | tf_op | source)
XLA Modules:
  0.0 60.9 jit_solution(11554565419820973399)
XLA Ops:
  0.0 0.7 %exp.3 = f32[32]{0:T(128)S(1)} exponential(f32[32]{0:T(128)} %param.30) | non-fusion elementwise | bytes 256 | tf_op jit(solution)/shard_map/exp | solution.py:49
  0.7 1.6 %multiply_add_fusion = (f32[32,64]{1,0:T(8,128)}, f32[32,64]{1,0:T(8,128)S(1)}, f32[32,64]{1,0:T(8,128)S(1)}, f32[32,64]{1,0:T(8,128)}, f32[32,64]{1,0:T(8,128)}) fusion(f32[32,64]{1,0:T(8,128)} %param.29, f32[32,64]{1,0:T(8,128)} %param.28, f32[32]{0:T(128)S(1)} %exp.3), kind=kLoop, calls=%fused_computation | loop fusion | flops 47104 | bytes 57472 | tf_op jit(solution)/shard_map/add | solution.py:61
  2.2 0.6 multiply_subtract_fusion.factor_r_ref
  2.8 56.0 %layer.1 = bf16[192,2048]{1,0:T(8,128)(2,1)} custom-call(bf16[192,2048]{1,0:T(8,128)(2,1)} %tokens_ref.1, f32[1,2048]{1,0:T(1,128)} %bitcast.17, bf16[2048,512]{1,0:T(8,128)(2,1)} %w_input_ref.1, bf16[2048,512]{1,0:T(8,128)(2,1)} %w_query_ref.1, bf16[2048,512]{1,0:T(8,128)(2,1)} %w_key_ref.1, bf16[2048,512]{1,0:T(8,128)(2,1)} %w_value_ref.1, ...), custom_call_target="tpu_custom_call" | custom-call | tf_op jit(solution)/shard_map/layer/pallas_call | solution.py:774
  58.8 2.1 %copy.21 = bf16[192,2048]{1,0:T(8,128)(2,1)} copy(bf16[192,2048]{1,0:T(8,128)(2,1)} %layer.1) | data formatting | bytes 1572864
where the time goes:
time: 61.3 us; the launch traced here: 60.9 us
  Pallas kernels  56 us (91%)
  local copies, waits for them, and re-layouts  2.75 us (4%)
  other arithmetic  2.16 us (4%)
    pallas_call x1, Pallas kernels, layer(): pl.pallas_call(functools.partial(mixer_kernel, ranks), out_shape=jax.Shap...  56 us
    unnamed x1, local copies, waits for them, and re-layouts  2.09 us
    add x1, other arithmetic, discretize(): factor_r[..., None] * input_imag + factor_i[..., None] * input_real  1.56 us

commit v1 on v0

--- a/solution.py
+++ b/solution.py
@@ -320,6 +320,39 @@
     return out_r, out_i
 
 
+LOG2E = 1.4426950408889634
+OWNERS = (0, 1, 1, 2)
+
+
+def owned_span(owner):
+    held = [pair for pair, rank in enumerate(OWNERS) if rank == owner]
+    return (held[0], held[-1] + 1) if held else (0, 0)
+
+
+def routes():
+    early, late, onward = [], [], []
+    for kind in ("k", "v"):
+        early.append((kind, 0, 1, 0, owned_span(2)))
+        early.append((kind, 1, 2, 1, owned_span(2)))
+        early.append((kind, 1, 0, 1, owned_span(0)))
+        early.append((kind, 2, 3, 0, (0, len(OWNERS))))
+        late.append((kind, 0, 1, 0, owned_span(1)))
+        late.append((kind, 0, 1, 0, owned_span(0)))
+        onward.append((kind, 1, 2, 0, owned_span(2)))
+    for slot in range(2):
+        for owner in range(3):
+            if owner != slot + 2:
+                early.append(("q", slot + 2, owner, slot, owned_span(owner)))
+    biases = [("b", 0, 1, 0), ("b", 1, 0, 1), ("b", 0, 2, 0), ("b", 1, 2, 1), ("b", 2, 3, 0)]
+    keep = [[route for route in group if route[4][0] < route[4][1]] for group in (early, late, onward)]
+    return keep[0], keep[1], keep[2], biases
+
+
+def route_count():
+    early, late, onward, biases = routes()
+    return 2 * len(early) + len(late) + len(onward) + len(biases)
+
+
 def mixer_kernel(
     ranks,
     tokens_ref,
@@ -360,24 +393,24 @@
     row_sem,
     part_send,
     part_recv,
-    q_land,
-    k_land,
-    v_land,
-    bias_land,
+    q_far,
+    k_far,
+    v_far,
+    bias_far,
     push_r,
     push_i,
     up_ref,
     seg_r,
     seg_i,
     ends_land,
-    q_two,
-    acc_ref,
-    run_ref,
-    out_stage,
-    out_land,
-    local_sem,
-    send_sem,
-    recv_sem,
+    acc_own,
+    run_own,
+    acc_far,
+    run_far,
+    far_stage,
+    far_land,
+    route_send,
+    route_recv,
     end_send,
     end_recv,
     back_send,
@@ -386,6 +419,7 @@
     rows, width = u_ref.shape
     states = decay_ref.shape[1]
     chunks = rows // LANES
+    pairs = width // LANES
     seg_len = rows // 8
     own_count, features = tokens_ref.shape
     core = lax.axis_index("tp")
@@ -420,20 +454,75 @@
     mean = jnp.sum(token_rows * token_rows, axis=-1, keepdims=True) * (1.0 / features)
     scaled = token_rows * lax.rsqrt(mean + EPSILON) * norm_gain_ref[...]
     normed[own_rows, :] = scaled.astype(jnp.bfloat16)
-    bias = bias_ref[...].astype(jnp.float32)
-    for rank in range(ranks):
-        for chunk in range(chunks):
-            bias_stage[rank, chunk] = bias[
-                2 * rank : 2 * rank + 2, chunk * LANES : (chunk + 1) * LANES
+    bias = bias_ref[...].astype(jnp.float32) * LOG2E
+    for chunk in range(chunks):
+        for head in range(2 * pairs):
+            lanes = slice((head % 2) * LANES, (head % 2 + 1) * LANES)
+            bias_stage[chunk, head // 2 : head // 2 + 1, lanes] = bias[
+                head : head + 1, chunk * LANES : (chunk + 1) * LANES
             ]
     q_gain, k_gain = (
         jnp.concatenate([ref[...], ref[...]], axis=1) for ref in (q_gain_ref, k_gain_ref)
     )
+    q_gain = q_gain * (LOG2E * HEAD_DIM**-0.5)
     groups = decay_r_ref.shape[0]
     for row, ref in enumerate((decay_r_ref, decay_i_ref)):
         decay_ref[row : row + 1, :] = jnp.concatenate(
             [ref[group : group + 1, :] for group in range(groups)], axis=1
         )
+
+    early, late, onward, biases = routes()
+    sources = {"q": q_norm, "k": k_norm, "v": v_ref}
+    targets = {"q": q_far, "k": k_far, "v": v_far}
+    issued = []
+
+    def make_route(ident, route, at, relay=False):
+        kind, origin, goal, slot = route[:4]
+        if kind == "b":
+            source, target = bias_stage, bias_far.at[slot]
+        else:
+            cols = slice(route[4][0] * LANES, route[4][1] * LANES)
+            target = targets[kind].at[slot, at, cols]
+            source = target if relay else sources[kind].at[at, cols]
+        return pltpu.make_async_remote_copy(
+            src_ref=source,
+            dst_ref=target,
+            send_sem=route_send.at[ident],
+            recv_sem=route_recv.at[ident],
+            device_id={"sp": goal},
+            device_id_type=pl.DeviceIdType.MESH,
+        )
+
+    def start_routes(chosen, at, relay=False):
+        entries = []
+        for route in chosen:
+            entries.append((len(issued), route, make_route(len(issued), route, at, relay)))
+            issued.append((route, entries[-1][2]))
+        for origin in range(ranks):
+            sent = [copy for _, route, copy in entries if route[1] == origin]
+            if sent:
+
+                @pl.when(me == origin)
+                def _(sent=sent):
+                    for copy in sent:
+                        copy.start()
+
+    waited = set()
+
+    def wait_routes(test):
+        for goal in range(ranks):
+            due = [
+                index
+                for index, (route, _) in enumerate(issued)
+                if route[2] == goal and index not in waited and test(route)
+            ]
+            waited.update(due)
+            if due:
+
+                @pl.when(me == goal)
+                def _(due=due):
+                    for index in due:
+                        issued[index][1].wait_recv()
 
     pl.semaphore_wait(barrier, ranks)
     row_copy = pltpu.make_async_remote_copy(
@@ -444,6 +533,7 @@
         **mate,
     )
     row_copy.start()
+    start_routes(biases, None)
 
     def project(slot, at):
         flat = dot_nn(normed[at, :], w_held[slot]).astype(jnp.bfloat16)
@@ -452,53 +542,24 @@
         elif slot == 3:
             u_ref[at, :] = flat
         else:
-            gain, target, scale = (
-                (k_gain, k_norm, 1.0) if slot == 0 else (q_gain, q_norm, HEAD_DIM**-0.5)
-            )
+            gain, target = (k_gain, k_norm) if slot == 0 else (q_gain, q_norm)
             for tile in range(width // LANES):
                 cols = slice(tile * LANES, (tile + 1) * LANES)
                 part = head_rms(flat[:, cols].astype(jnp.float32)) * gain
-                target[at, cols] = part.astype(jnp.bfloat16) * jnp.bfloat16(scale)
-
-    for slot in range(4):
+                target[at, cols] = part.astype(jnp.bfloat16)
+
+    for slot, kind in enumerate("kvq"):
         weights[slot].wait()
         project(slot, own_rows)
+        start_routes([route for route in early if route[0] == kind], own_rows)
     row_copy.wait_recv()
-
-    my_rows = pl.ds(pl.multiple_of(me * rows, rows), rows)
-
-    def piece(kind, rank):
-        cols = pl.ds(pl.multiple_of(rank * LANES, LANES), LANES)
-        if kind == 3:
-            return bias_stage.at[rank], bias_land.at[pl.ds(me * chunks, chunks)]
-        source, target = ((k_norm, k_land), (v_ref, v_land), (q_norm, q_land))[kind]
-        return source.at[:, cols], target.at[my_rows, :]
-
-    sends = []
-    local = []
-
-    def redistribute(kind):
-        for step in others:
-            source, target = piece(kind, at_rank(step))
-            copy = pltpu.make_async_remote_copy(
-                src_ref=source,
-                dst_ref=target,
-                send_sem=send_sem.at[step, kind],
-                recv_sem=recv_sem.at[step, kind],
-                device_id={"sp": at_rank(step)},
-                device_id_type=pl.DeviceIdType.MESH,
-            )
-            copy.start()
-            sends.append(copy)
-        source, target = piece(kind, me)
-        copy = pltpu.make_async_copy(source, target, local_sem.at[kind])
-        copy.start()
-        local.append(copy)
-
-    redistribute(3)
-    project(0, mate_rows)
-    redistribute(0)
-    project(3, mate_rows)
+    for slot, kind in enumerate("kvq"):
+        project(slot, mate_rows)
+        start_routes([route for route in early if route[0] == kind], mate_rows)
+    whole = slice(0, rows)
+    start_routes(late, whole)
+    weights[3].wait()
+    project(3, whole)
 
     def place(axis):
         index = lax.broadcasted_iota(jnp.int32, (rows, rows), axis)
@@ -588,10 +649,157 @@
         copy.start()
         end_copies.append(copy)
 
-    project(1, mate_rows)
-    redistribute(1)
-    project(2, mate_rows)
-    redistribute(2)
+    tail = lax.broadcasted_iota(jnp.int32, (2 * LANES, 2 * LANES), 0)
+    col = lax.broadcasted_iota(jnp.int32, (2 * LANES, 2 * LANES), 1)
+    tail = jnp.where(
+        jnp.logical_and(tail >= col, tail // LANES == col // LANES), 1.0, 0.0
+    ).astype(jnp.bfloat16)
+    lane = lax.broadcasted_iota(jnp.int32, (1, LANES), 1)
+    low_mask = jnp.where(lane < HEAD_DIM, 1.0, 0.0).astype(jnp.bfloat16)
+    high_mask = jnp.where(lane < HEAD_DIM, 0.0, 1.0).astype(jnp.bfloat16)
+
+    def both_heads(block):
+        return jnp.concatenate([block * low_mask, block * high_mask], axis=0)
+
+    def attend(queries, keys, values, bias_row, running, diagonal):
+        count = queries.shape[0]
+        z = dot_nt(queries, both_heads(keys)) + bias_row
+        soft = jnp.log(1.0 + jnp.exp2(z)) * LOG2E
+        if diagonal:
+            causal = (lax.broadcasted_iota(jnp.int32, z.shape, 1) & (LANES - 1)) < (
+                lax.broadcasted_iota(jnp.int32, z.shape, 0)
+            )
+            soft = jnp.where(causal, soft, 0.0)
+        sums = dot_nn(soft.astype(jnp.bfloat16), tail)
+        weight = jnp.exp2(z - (sums + running))
+        if diagonal:
+            weight = jnp.where(causal, weight, 0.0)
+        totals = jnp.concatenate(
+            [
+                jnp.broadcast_to(sums[:, :1], (count, LANES)),
+                jnp.broadcast_to(sums[:, LANES : LANES + 1], (count, LANES)),
+            ],
+            axis=1,
+        )
+        part = dot_nn(weight.astype(jnp.bfloat16), both_heads(values))
+        return part, running + totals
+
+    def pair_cols(pair):
+        return pl.ds(pl.multiple_of(pair * LANES, LANES), LANES)
+
+    def run_cols(pair):
+        return pl.ds(pl.multiple_of(pair * 2 * LANES, 2 * LANES), 2 * LANES)
+
+    def own_pair(pair, carry):
+        cols, wide = pair_cols(pair), run_cols(pair)
+        acc_own[:, cols] = jnp.zeros((rows, LANES), jnp.float32)
+        run_own[:, wide] = jnp.zeros((rows, 2 * LANES), jnp.float32)
+        for chunk in reversed(range(chunks)):
+            at = slice(chunk * LANES, (chunk + 1) * LANES)
+            below = slice(chunk * LANES, rows)
+            part, running = attend(
+                q_norm[below, cols],
+                k_norm[at, cols],
+                v_ref[at, cols],
+                bias_stage[chunk, pl.ds(pair, 1), :],
+                run_own[below, wide],
+                True,
+            )
+            acc_own[below, cols] += part
+            run_own[below, wide] = running
+        return carry
+
+    def near_pair(pair, carry):
+        cols, wide = pair_cols(pair), run_cols(pair)
+        for chunk in reversed(range(chunks)):
+            at = slice(chunk * LANES, (chunk + 1) * LANES)
+            part, running = attend(
+                q_norm[:, cols],
+                k_far[0, at, cols],
+                v_far[0, at, cols],
+                bias_far[0, chunk, pl.ds(pair, 1), :],
+                run_own[:, wide],
+                False,
+            )
+            acc_own[:, cols] += part
+            run_own[:, wide] = running
+        return carry
+
+    def far_copy(slot, pair):
+        return pltpu.make_async_remote_copy(
+            src_ref=far_stage.at[slot, :, pair_cols(pair)],
+            dst_ref=far_land.at[:, pair_cols(pair)],
+            send_sem=back_send.at[slot, pair],
+            recv_sem=back_recv.at[pair],
+            device_id={"sp": slot + 2},
+            device_id_type=pl.DeviceIdType.MESH,
+        )
+
+    def far_pair(pair, carry):
+        cols = pair_cols(pair)
+        queries = q_far[:, :, cols].reshape(2 * rows, LANES)
+        acc_far[...] = jnp.zeros_like(acc_far)
+        run_far[...] = jnp.zeros_like(run_far)
+
+        def key_block(step, inner):
+            slot = 1 - step
+            for chunk in reversed(range(chunks)):
+                at = slice(chunk * LANES, (chunk + 1) * LANES)
+                part, running = attend(
+                    queries,
+                    k_far[slot, at, cols],
+                    v_far[slot, at, cols],
+                    bias_far[slot, chunk, pl.ds(pair, 1), :],
+                    run_far[...],
+                    False,
+                )
+                acc_far[...] += part
+                run_far[...] = running
+            return inner
+
+        lax.fori_loop(0, 2, key_block, 0)
+        for slot in range(2):
+            part = acc_far[slot * rows : (slot + 1) * rows, :].astype(jnp.bfloat16)
+
+            @pl.when(me == slot + 2)
+            def _(part=part):
+                far_land[:, cols] = part
+
+            @pl.when(me != slot + 2)
+            def _(part=part, slot=slot):
+                far_stage[slot, :, cols] = part
+                far_copy(slot, pair).start()
+
+        return carry
+
+    first_pair, last_pair = jnp.int32(0), jnp.int32(0)
+    for owner in range(3):
+        first_pair = jnp.where(me == owner, owned_span(owner)[0], first_pair)
+        last_pair = jnp.where(me == owner, owned_span(owner)[1], last_pair)
+
+    if onward:
+        wait_routes(lambda route: route[2] == 1 and route[0] in "kv" and route[4] == owned_span(2))
+        start_routes(onward, whole, True)
+    lax.fori_loop(0, pairs, own_pair, 0)
+    for owner, (slot, held, kept) in enumerate(
+        (
+            (0, ((k_norm, k_far), (v_ref, v_far), (bias_stage, bias_far)), None),
+            (1, ((k_norm, k_far), (v_ref, v_far), (bias_stage, bias_far)), None),
+            (0, ((q_norm, q_far),), None),
+        )
+    ):
+        @pl.when(me == owner)
+        def _(slot=slot, held=held):
+            for source, target in held:
+                target[slot] = source[...]
+
+    wait_routes(lambda route: route[2] < 3)
+    lax.fori_loop(first_pair, last_pair, far_pair, 0)
+    wait_routes(lambda route: True)
+
+    @pl.when(lax.rem(me, 2) == 1)
+    def _():
+        lax.fori_loop(0, pairs, near_pair, 0)
 
     for copy in end_copies:
         copy.wait_recv()
@@ -643,85 +851,26 @@
 
     lax.fori_loop(0, pieces, state_piece, 0)
 
-    for copy in local:
-        copy.wait()
-    for copy in sends:
-        copy.wait_recv()
-
-    tail = lax.broadcasted_iota(jnp.int32, (LANES, 2 * LANES), 0)
-    col = lax.broadcasted_iota(jnp.int32, (LANES, 2 * LANES), 1)
-    tail = jnp.where(jnp.logical_or(tail >= col, col >= LANES), 1.0, 0.0).astype(jnp.bfloat16)
-    lane = lax.broadcasted_iota(jnp.int32, (1, LANES), 1)
-    low_mask = jnp.where(lane < HEAD_DIM, 1.0, 0.0).astype(jnp.bfloat16)
-    high_mask = jnp.where(lane < HEAD_DIM, 0.0, 1.0).astype(jnp.bfloat16)
-
-    def chunk_step(chunk, first, diagonal):
-        count = rows - first
-        at = pl.ds(pl.multiple_of(chunk * LANES, LANES), LANES)
-        keys = k_land[at, :]
-        values = v_land[at, :]
-        values = jnp.concatenate([values * low_mask, values * high_mask], axis=0)
-        probs = []
-        for head in range(2):
-            span_rows = slice(head * rows + first, (head + 1) * rows)
-            z = dot_nt(q_two[span_rows, :], keys) + bias_land[chunk, head : head + 1, :]
-            keep = jnp.minimum(-z, 0.0) - jnp.log(1.0 + jnp.exp(-jnp.abs(z)))
-            if diagonal:
-                causal = lax.broadcasted_iota(
-                    jnp.int32, (count, LANES), 1
-                ) < lax.broadcasted_iota(jnp.int32, (count, LANES), 0)
-                keep = jnp.where(causal, keep, 0.0)
-            sums = dot_nn(keep.astype(jnp.bfloat16), tail)
-            running = run_ref[span_rows, :]
-            weight = jnp.exp(z + sums[:, :LANES] + running)
-            if diagonal:
-                weight = jnp.where(causal, weight, 0.0)
-            run_ref[span_rows, :] = running + sums[:, LANES:]
-            probs.append(weight.astype(jnp.bfloat16))
-        acc_ref[first:, :] += dot_nn(jnp.concatenate(probs, axis=1), values)
-
-    def back_copy(step):
-        rank = at_rank(step)
-        return pltpu.make_async_remote_copy(
-            src_ref=out_stage.at[rank],
-            dst_ref=out_land.at[me],
-            send_sem=back_send.at[step],
-            recv_sem=back_recv.at[step],
-            device_id={"sp": rank},
-            device_id_type=pl.DeviceIdType.MESH,
-        )
-
-    def query_block(step, carry):
-        rank = at_rank(step)
-        queries = q_land[pl.ds(pl.multiple_of(rank * rows, rows), rows), :]
-        q_two[:rows, :] = queries * low_mask
-        q_two[rows:, :] = queries * high_mask
-        acc_ref[...] = jnp.zeros_like(acc_ref)
-        run_ref[...] = jnp.zeros_like(run_ref)
-        for part in reversed(range(chunks)):
-            chunk_step(rank * chunks + part, part * LANES, True)
-
-        def earlier(index, inner):
-            for part in reversed(range(chunks)):
-                chunk_step((rank - 1 - index) * chunks + part, 0, False)
-            return inner
-
-        lax.fori_loop(0, rank, earlier, 0)
-        out_stage[rank] = head_rms(acc_ref[...]).astype(jnp.bfloat16)
-
-        @pl.when(step < ranks)
-        def _():
-            back_copy(step).start()
-
-        return carry
-
-    lax.fori_loop(1, ranks + 1, query_block, 0)
-
-    out_land[me] = out_stage[me]
-    for step in others:
-        back_copy(step).wait_recv()
-    for rank in range(ranks):
-        act_ref[:, width + rank * LANES : width + (rank + 1) * LANES] = out_land[rank]
+    for pair in range(pairs):
+        cols = slice(pair * LANES, (pair + 1) * LANES)
+        for goal in range(2, ranks):
+            if OWNERS[pair] != goal:
+
+                @pl.when(me == goal)
+                def _(pair=pair):
+                    far_copy(0, pair).wait_recv()
+
+        @pl.when(me >= 2)
+        def _(pair=pair, cols=cols):
+            low = run_own[:, 2 * pair * LANES : (2 * pair + 1) * LANES]
+            high = run_own[:, (2 * pair + 1) * LANES : (2 * pair + 2) * LANES]
+            factor = jnp.exp2(-by_head(low, high, low.shape))
+            acc_own[:, cols] += factor * far_land[:, cols].astype(jnp.float32)
+
+        act_ref[:, width + pair * LANES : width + (pair + 1) * LANES] = head_rms(
+            acc_own[:, cols]
+        ).astype(jnp.bfloat16)
+
     def part_copy(index):
         return pltpu.make_async_remote_copy(
             src_ref=out_part.at[index],
@@ -752,10 +901,24 @@
     row_copy.wait_send()
     for index in range(pieces):
         part_copy(index).wait_send()
-    for copy in sends + end_copies:
+    for copy in end_copies:
         copy.wait_send()
-    for step in others:
-        back_copy(step).wait_send()
+    for origin in range(ranks):
+        sent = [copy for route, copy in issued if route[1] == origin]
+        if sent:
+
+            @pl.when(me == origin)
+            def _(sent=sent):
+                for copy in sent:
+                    copy.wait_send()
+
+    for pair in range(pairs):
+        for slot in range(2):
+            if OWNERS[pair] != slot + 2:
+
+                @pl.when(me == OWNERS[pair])
+                def _(pair=pair, slot=slot):
+                    far_copy(slot, pair).wait_send()
 
 
 def layer(ranks, tokens, norm_gain, weights, gains, key_bias, plan):
@@ -764,6 +927,7 @@
     rows = key_bias.shape[0]
     states = plan[0].size
     chunks = rows // LANES
+    pairs = width // LANES
     pieces = features // 512
     bias = key_bias.T
     gains = [gain[None, :] for gain in gains]
@@ -787,35 +951,35 @@
             pltpu.VMEM((rows, width), half),
             pltpu.VMEM((rows, width), half),
             pltpu.VMEM((rows, width), half),
-            pltpu.VMEM((ranks, chunks, 2, LANES), full),
+            pltpu.VMEM((chunks, pairs, 2 * LANES), full),
             pltpu.VMEM((pieces, count, 512), half),
             pltpu.VMEM((pieces, count, 512), half),
             dma((6,)),
             dma((2,)),
             dma((pieces,)),
             dma((pieces,)),
-            pltpu.VMEM((ranks * rows, LANES), half),
-            pltpu.VMEM((ranks * rows, LANES), half),
-            pltpu.VMEM((ranks * rows, LANES), half),
-            pltpu.VMEM((ranks * chunks, 2, LANES), full),
+            pltpu.VMEM((2, rows, width), half),
+            pltpu.VMEM((2, rows, width), half),
+            pltpu.VMEM((2, rows, width), half),
+            pltpu.VMEM((2, chunks, pairs, 2 * LANES), full),
             pltpu.VMEM((rows, states), full),
             pltpu.VMEM((rows, states), full),
             pltpu.VMEM((rows, width), half),
             pltpu.VMEM((8, states), full),
             pltpu.VMEM((8, states), full),
             pltpu.VMEM((ranks, 2, states), full),
-            pltpu.VMEM((2 * rows, LANES), half),
-            pltpu.VMEM((rows, LANES), full),
+            pltpu.VMEM((rows, width), full),
+            pltpu.VMEM((rows, 2 * width), full),
             pltpu.VMEM((2 * rows, LANES), full),
-            pltpu.VMEM((ranks, rows, LANES), half),
-            pltpu.VMEM((ranks, rows, LANES), half),
-            dma((4,)),
-            dma((ranks, 4)),
-            dma((ranks, 4)),
+            pltpu.VMEM((2 * rows, 2 * LANES), full),
+            pltpu.VMEM((2, rows, width), half),
+            pltpu.VMEM((rows, width), half),
+            dma((route_count(),)),
+            dma((route_count(),)),
             dma((ranks,)),
             dma((ranks,)),
-            dma((ranks + 1,)),
-            dma((ranks + 1,)),
+            dma((2, pairs)),
+            dma((pairs,)),
         ],
         compiler_params=pltpu.CompilerParams(
             collective_id=0, has_side_effects=True, vmem_limit_bytes=58 * 2**20
@@ -849,7 +1013,7 @@
     width = w_query.shape[1]
     rows = key_bias.shape[0]
     fits = (
-        ranks > 1
+        ranks == len(OWNERS)
         and width == ranks * LANES
         and w_input.shape[1] == width
         and width % 256 == 0

time: 61.3 us -> 51.6 us (0.84)
  the two profiles are of different devices: /device:TPU:0 before, /device:TPU:11 now
where the time goes in v1:
time: 51.6 us; the launch traced here: 51.2 us
  Pallas kernels  46.3 us (90%)
  local copies, waits for them, and re-layouts  2.75 us (5%)
  other arithmetic  2.16 us (4%)
    pallas_call x1, Pallas kernels, layer(): pl.pallas_call(functools.partial(mixer_kernel, ranks), out_shape=jax.Shap...  46.3 us
    unnamed x1, local copies, waits for them, and re-layouts  2.09 us
    add x1, other arithmetic, discretize(): factor_r[..., None] * input_imag + factor_i[..., None] * input_real  1.56 us

profile of v1, /device:TPU:11, one launch (start us, length us, event | category | flops | bytes accessed | tf_op | source)
XLA Modules:
  0.0 51.2 jit_solution(10518589751752721219)
XLA Ops:
  0.0 0.7 %exp.3 = f32[32]{0:T(128)S(1)} exponential(f32[32]{0:T(128)} %param.30) | non-fusion elementwise | bytes 256 | tf_op jit(solution)/shard_map/exp | solution.py:49
  0.7 1.6 %multiply_add_fusion = (f32[32,64]{1,0:T(8,128)}, f32[32,64]{1,0:T(8,128)S(1)}, f32[32,64]{1,0:T(8,128)S(1)}, f32[32,64]{1,0:T(8,128)}, f32[32,64]{1,0:T(8,128)}) fusion(f32[32,64]{1,0:T(8,128)} %param.29, f32[32,64]{1,0:T(8,128)} %param.28, f32[32]{0:T(128)S(1)} %exp.3), kind=kLoop, calls=%fused_computation | loop fusion | flops 47104 | bytes 57472 | tf_op jit(solution)/shard_map/add | solution.py:61
  2.2 0.6 %multiply_subtract_fusion.factor_r_ref = f32[32,64]{1,0:T(8,128)} fusion(f32[32,64]{1,0:T(8,128)S(1)} %get-tuple-element.7, f32[32,64]{1,0:T(8,128)S(1)} %get-tuple-element.6), kind=kLoop, calls=%fused_computation.1 | loop fusion | flops 4096 | bytes 24576 | tf_op jit(solution)/shard_map/sub | solution.py:60
  2.8 46.3 %layer.1 = bf16[192,2048]{1,0:T(8,128)(2,1)} custom-call(bf16[192,2048]{1,0:T(8,128)(2,1)} %tokens_ref.1, f32[1,2048]{1,0:T(1,128)} %bitcast.17, bf16[2048,512]{1,0:T(8,128)(2,1)} %w_input_ref.1, bf16[2048,512]{1,0:T(8,128)(2,1)} %w_query_ref.1, bf16[2048,512]{1,0:T(8,128)(2,1)} %w_key_ref.1, bf16[2048,512]{1,0:T(8,128)(2,1)} %w_value_ref.1, ...), custom_call_target="tpu_custom_call" | custom-call | tf_op jit(solution)/shard_map/layer/pallas_call | solution.py:938
  49.2 2.1 %copy.21 = bf16[192,2048]{1,0:T(8,128)(2,1)} copy(bf16[192,2048]{1,0:T(8,128)(2,1)} %layer.1) | data formatting | bytes 1572864

commit v2 on v0

--- a/solution.py
+++ b/solution.py
@@ -45,7 +45,7 @@
     return (prod_r, prod_i, state_r, state_i)
 
 
-def discretize(eigen_real, eigen_imag, log_step, input_real, input_imag):
+def plain_discretize(eigen_real, eigen_imag, log_step, input_real, input_imag):
     step_size = jnp.exp(log_step)[:, None]
     rotation = eigen_imag * step_size
     shrink = jnp.expm1(eigen_real * step_size)
@@ -179,7 +179,7 @@
     read_imag,
     skip_gain,
 ):
-    decay_r, decay_i, drive_r, drive_i = discretize(
+    decay_r, decay_i, drive_r, drive_i = plain_discretize(
         eigen_real, eigen_imag, log_step, input_real, input_imag
     )
     row_count = inputs.shape[0]
@@ -320,6 +320,69 @@
     return out_r, out_i
 
 
+LOG2E = 1.4426950408889634
+OWNERS = (0, 1, 1, 2)
+KINDS = "kvq"
+
+
+def pairs_of(owner):
+    return [pair for pair, rank in reversed(list(enumerate(OWNERS))) if rank == owner]
+
+
+LATE = 2
+
+
+def routes(kind, origin, late=0):
+    every = list(reversed(range(len(OWNERS))))
+    if late == 1:
+        plan = {0: [(1, 0, pairs_of(1))]}
+    elif late == 2:
+        plan = {0: [(1, 0, pairs_of(0))], 2: [(3, 0, every[LATE:])]}
+    elif kind == "q":
+        plan = {
+            2: [(0, 0, pairs_of(0)), (1, 0, pairs_of(1))],
+            3: [(0, 1, pairs_of(0)), (1, 1, pairs_of(1)), (2, 1, pairs_of(2))],
+        }
+    else:
+        plan = {
+            0: [(1, 0, pairs_of(2))],
+            1: [(2, 1, pairs_of(2)), (0, 1, pairs_of(0))],
+            2: [(3, 0, every[:LATE])],
+        }
+    return [(goal, slot, pair) for goal, slot, held in plan.get(origin, []) for pair in held]
+
+
+BIASES = ((0, 1, 0), (1, 0, 1), (0, 2, 0), (1, 2, 1), (2, 3, 0))
+
+
+def small_expm1(value):
+    series = jnp.ones_like(value)
+    for order in range(9, 1, -1):
+        series = 1.0 + value * series * (1.0 / order)
+    return jnp.where(value > -0.5, value * series, jnp.exp(value) - 1.0)
+
+
+def discretize(eigen_real, eigen_imag, log_step):
+    groups = eigen_real.shape[0]
+    diagonal = lax.broadcasted_iota(jnp.int32, (groups, groups), 0) == lax.broadcasted_iota(
+        jnp.int32, (groups, groups), 1
+    )
+    step_row = jnp.broadcast_to(jnp.exp(log_step), (groups, groups))
+    step_size = jnp.sum(jnp.where(diagonal, step_row, 0.0), axis=1, keepdims=True)
+    rotation = eigen_imag * step_size
+    shrink = small_expm1(eigen_real * step_size)
+    cosine = jnp.cos(rotation)
+    sine_part = jnp.sin(rotation)
+    half_sine = jnp.sin(0.5 * rotation)
+    decay_r = (1.0 + shrink) * cosine
+    decay_i = (1.0 + shrink) * sine_part
+    minus_r = shrink * cosine - 2.0 * half_sine * half_sine
+    modulus = eigen_real * eigen_real + eigen_imag * eigen_imag
+    factor_r = (minus_r * eigen_real + decay_i * eigen_imag) / modulus
+    factor_i = (decay_i * eigen_real - minus_r * eigen_imag) / modulus
+    return decay_r, decay_i, factor_r, factor_i
+
+
 def mixer_kernel(
     ranks,
     tokens_ref,
@@ -333,16 +396,16 @@
     q_gain_ref,
     k_gain_ref,
     bias_ref,
-    decay_r_ref,
-    decay_i_ref,
-    factor_r_ref,
-    factor_i_ref,
+    eigen_r_ref,
+    eigen_i_ref,
+    log_step_ref,
     input_r_ref,
     input_i_ref,
     read_r_ref,
     read_i_ref,
     skip_ref,
     out_ref,
+    plan_ref,
     normed,
     decay_ref,
     state_part,
@@ -360,24 +423,26 @@
     row_sem,
     part_send,
     part_recv,
-    q_land,
-    k_land,
-    v_land,
-    bias_land,
+    q_far,
+    k_far,
+    v_far,
+    bias_far,
     push_r,
     push_i,
     up_ref,
     seg_r,
     seg_i,
     ends_land,
-    q_two,
-    acc_ref,
-    run_ref,
-    out_stage,
-    out_land,
-    local_sem,
-    send_sem,
-    recv_sem,
+    acc_own,
+    run_own,
+    acc_far,
+    run_far,
+    far_stage,
+    far_land,
+    route_send,
+    route_recv,
+    bias_send,
+    bias_recv,
     end_send,
     end_recv,
     back_send,
@@ -386,6 +451,7 @@
     rows, width = u_ref.shape
     states = decay_ref.shape[1]
     chunks = rows // LANES
+    pairs = width // LANES
     seg_len = rows // 8
     own_count, features = tokens_ref.shape
     core = lax.axis_index("tp")
@@ -413,27 +479,102 @@
     for slot, ref in enumerate((w_state_ref, w_attn_ref)):
         target = w_out.at[slot * width : (slot + 1) * width, :]
         weights.append(pltpu.make_async_copy(ref, target, w_sem.at[4 + slot]))
-    for copy in weights:
-        copy.start()
+    for low, order in ((True, (0, 1, 2)), (False, (2, 0, 1))):
+
+        @pl.when((me < 2) if low else (me >= 2))
+        def _(order=order):
+            for slot in order:
+                weights[slot].start()
+
 
     token_rows = tokens_ref[...].astype(jnp.float32)
     mean = jnp.sum(token_rows * token_rows, axis=-1, keepdims=True) * (1.0 / features)
     scaled = token_rows * lax.rsqrt(mean + EPSILON) * norm_gain_ref[...]
     normed[own_rows, :] = scaled.astype(jnp.bfloat16)
-    bias = bias_ref[...].astype(jnp.float32)
-    for rank in range(ranks):
-        for chunk in range(chunks):
-            bias_stage[rank, chunk] = bias[
-                2 * rank : 2 * rank + 2, chunk * LANES : (chunk + 1) * LANES
+    bias = bias_ref[...].astype(jnp.float32) * LOG2E
+    for chunk in range(chunks):
+        for head in range(2 * pairs):
+            lanes = slice((head % 2) * LANES, (head % 2 + 1) * LANES)
+            bias_stage[chunk, head // 2 : head // 2 + 1, lanes] = bias[
+                head : head + 1, chunk * LANES : (chunk + 1) * LANES
             ]
     q_gain, k_gain = (
         jnp.concatenate([ref[...], ref[...]], axis=1) for ref in (q_gain_ref, k_gain_ref)
     )
-    groups = decay_r_ref.shape[0]
-    for row, ref in enumerate((decay_r_ref, decay_i_ref)):
+    q_gain = q_gain * (LOG2E * HEAD_DIM**-0.5)
+    groups = eigen_r_ref.shape[0]
+    plan = discretize(eigen_r_ref[...], eigen_i_ref[...], log_step_ref[...])
+    for row, value in enumerate(plan):
+        plan_ref[row] = value
+    for row in range(2):
         decay_ref[row : row + 1, :] = jnp.concatenate(
-            [ref[group : group + 1, :] for group in range(groups)], axis=1
-        )
+            [plan_ref[row, group : group + 1, :] for group in range(groups)], axis=1
+        )
+
+    sources = (k_norm, v_ref, q_norm)
+    targets = (k_far, v_far, q_far)
+    sent = {rank: [] for rank in range(ranks)}
+
+    def piece_copy(kind, goal, slot, pair, part, relay=False):
+        at = (own_rows, mate_rows)[part]
+        cols = pair_cols(pair)
+        target = targets[kind].at[slot, at, cols]
+        return pltpu.make_async_remote_copy(
+            src_ref=target if relay else sources[kind].at[at, cols],
+            dst_ref=target,
+            send_sem=route_send.at[kind, int(relay), pair, part],
+            recv_sem=route_recv.at[kind, slot, pair, part],
+            device_id={"sp": goal},
+            device_id_type=pl.DeviceIdType.MESH,
+        )
+
+    def bias_copy(index):
+        _, goal, slot = BIASES[index]
+        return pltpu.make_async_remote_copy(
+            src_ref=bias_stage,
+            dst_ref=bias_far.at[slot],
+            send_sem=bias_send.at[index],
+            recv_sem=bias_recv.at[slot],
+            device_id={"sp": goal},
+            device_id_type=pl.DeviceIdType.MESH,
+        )
+
+    def send_entries(entries, origin):
+        sent[origin] += entries
+
+        @pl.when(me == origin)
+        def _():
+            for entry in entries:
+                piece_copy(*entry).start()
+
+    def send_pieces(kind, part, ranks_of):
+        for origin in ranks_of:
+            chosen = routes(KINDS[kind], origin)
+            if chosen:
+                send_entries([(kind, *route, part) for route in chosen], origin)
+
+    def send_late(ranks_of, late):
+        for origin in ranks_of:
+            chosen = routes("k", origin, late)
+            if chosen:
+                send_entries(
+                    [
+                        (kind, *route, part)
+                        for route in chosen
+                        for kind in range(2)
+                        for part in range(2)
+                    ],
+                    origin,
+                )
+
+    def arrive(kind, slot, pair):
+        for part in range(2):
+            piece_copy(kind, 0, slot, pair, part).wait_recv()
+
+    def pair_cols(pair):
+        if isinstance(pair, int):
+            return slice(pair * LANES, (pair + 1) * LANES)
+        return pl.ds(pl.multiple_of(pair * LANES, LANES), LANES)
 
     pl.semaphore_wait(barrier, ranks)
     row_copy = pltpu.make_async_remote_copy(
@@ -444,6 +585,15 @@
         **mate,
     )
     row_copy.start()
+    for copy in weights[3:]:
+        copy.start()
+    for index, (origin, _, _) in enumerate(BIASES):
+        sent[origin].append((index,))
+
+        @pl.when(me == origin)
+        def _(index=index):
+            bias_copy(index).start()
+
 
     def project(slot, at):
         flat = dot_nn(normed[at, :], w_held[slot]).astype(jnp.bfloat16)
@@ -452,53 +602,252 @@
         elif slot == 3:
             u_ref[at, :] = flat
         else:
-            gain, target, scale = (
-                (k_gain, k_norm, 1.0) if slot == 0 else (q_gain, q_norm, HEAD_DIM**-0.5)
-            )
+            gain, target = (k_gain, k_norm) if slot == 0 else (q_gain, q_norm)
             for tile in range(width // LANES):
                 cols = slice(tile * LANES, (tile + 1) * LANES)
                 part = head_rms(flat[:, cols].astype(jnp.float32)) * gain
-                target[at, cols] = part.astype(jnp.bfloat16) * jnp.bfloat16(scale)
-
-    for slot in range(4):
-        weights[slot].wait()
-        project(slot, own_rows)
+                target[at, cols] = part.astype(jnp.bfloat16)
+
+    low_order, high_order = (0, 1, 2), (2, 0, 1)
+
+    def project_part(part, at):
+        for ranks_of, order in (((0, 1), low_order), ((2, 3), high_order)):
+            @pl.when((me < 2) if order is low_order else (me >= 2))
+            def _(ranks_of=ranks_of, order=order):
+                for kind in order:
+                    if part == 0:
+                        weights[kind].wait()
+                    project(kind, at)
+                    send_pieces(kind, part, ranks_of)
+                if part == 1 and 0 in ranks_of:
+                    send_late((0,), 1)
+
+    project_part(0, own_rows)
     row_copy.wait_recv()
-
-    my_rows = pl.ds(pl.multiple_of(me * rows, rows), rows)
-
-    def piece(kind, rank):
-        cols = pl.ds(pl.multiple_of(rank * LANES, LANES), LANES)
-        if kind == 3:
-            return bias_stage.at[rank], bias_land.at[pl.ds(me * chunks, chunks)]
-        source, target = ((k_norm, k_land), (v_ref, v_land), (q_norm, q_land))[kind]
-        return source.at[:, cols], target.at[my_rows, :]
-
-    sends = []
-    local = []
-
-    def redistribute(kind):
-        for step in others:
-            source, target = piece(kind, at_rank(step))
-            copy = pltpu.make_async_remote_copy(
-                src_ref=source,
-                dst_ref=target,
-                send_sem=send_sem.at[step, kind],
-                recv_sem=recv_sem.at[step, kind],
-                device_id={"sp": at_rank(step)},
-                device_id_type=pl.DeviceIdType.MESH,
+    project_part(1, mate_rows)
+    whole = slice(0, rows)
+    tail = lax.broadcasted_iota(jnp.int32, (2 * LANES, 2 * LANES), 0)
+    col = lax.broadcasted_iota(jnp.int32, (2 * LANES, 2 * LANES), 1)
+    tail = jnp.where(
+        jnp.logical_and(tail >= col, tail // LANES == col // LANES), 1.0, 0.0
+    ).astype(jnp.bfloat16)
+    lane = lax.broadcasted_iota(jnp.int32, (1, LANES), 1)
+    low_mask = jnp.where(lane < HEAD_DIM, 1.0, 0.0).astype(jnp.bfloat16)
+    high_mask = jnp.where(lane < HEAD_DIM, 0.0, 1.0).astype(jnp.bfloat16)
+
+    def both_heads(block):
+        return jnp.concatenate([block * low_mask, block * high_mask], axis=0)
+
+    def attend(streams):
+        scores, softs, masks, sums = [], [], [], []
+        for queries, blocks, _, diagonal in streams:
+            for keys, _, bias_row, first in blocks:
+                z = dot_nt(queries[first:], both_heads(keys)) + bias_row
+                scores.append(z)
+                if diagonal:
+                    masks.append(
+                        (lax.broadcasted_iota(jnp.int32, z.shape, 1) & (LANES - 1))
+                        < lax.broadcasted_iota(jnp.int32, z.shape, 0)
+                    )
+                else:
+                    masks.append(None)
+        for z, mask in zip(scores, masks):
+            soft = jnp.log(1.0 + jnp.exp2(z)) * LOG2E
+            if mask is not None:
+                soft = jnp.where(mask, soft, 0.0)
+            softs.append(soft.astype(jnp.bfloat16))
+        for soft in softs:
+            sums.append(dot_nn(soft, tail))
+        results = []
+        at = 0
+        for queries, blocks, running, diagonal in streams:
+            probs, values, out = [], [], None
+            for _, block, _, first in blocks:
+                z, mask, inner = scores[at], masks[at], sums[at]
+                at += 1
+                count = z.shape[0]
+                if running.shape[0] < count:
+                    fresh = jnp.zeros((count - running.shape[0], 2 * LANES), jnp.float32)
+                    running = jnp.concatenate([fresh, running], axis=0)
+                weight = jnp.exp2(z - (inner + running))
+                if mask is not None:
+                    weight = jnp.where(mask, weight, 0.0)
+                totals = [
+                    jnp.broadcast_to(inner[:, head * LANES : head * LANES + 1], (count, LANES))
+                    for head in range(2)
+                ]
+                running = running + jnp.concatenate(totals, axis=1)
+                if diagonal:
+                    part = dot_nn(weight.astype(jnp.bfloat16), both_heads(block))
+                    if out is not None:
+                        fresh = part.shape[0] - out.shape[0]
+                        part = jnp.concatenate([part[:fresh], part[fresh:] + out], axis=0)
+                    out = part
+                else:
+                    probs.append(weight.astype(jnp.bfloat16))
+                    values.append(both_heads(block))
+            if not diagonal:
+                out = dot_nn(jnp.concatenate(probs, axis=1), jnp.concatenate(values, axis=0))
+            results.append((out, running))
+        return results
+
+    def run_cols(pair):
+        return pl.ds(pl.multiple_of(pair * 2 * LANES, 2 * LANES), 2 * LANES)
+
+    group = 2
+
+    def own_group(step, carry):
+        held = [step * group + index for index in range(group)]
+        streams = []
+        for pair in held:
+            cols = pair_cols(pair)
+            blocks = [
+                (
+                    k_norm[chunk * LANES : (chunk + 1) * LANES, cols],
+                    v_ref[chunk * LANES : (chunk + 1) * LANES, cols],
+                    bias_stage[chunk, pl.ds(pair, 1), :],
+                    chunk * LANES,
+                )
+                for chunk in reversed(range(chunks))
+            ]
+            none = jnp.zeros((LANES, 2 * LANES), jnp.float32)
+            streams.append((q_norm[:, cols], blocks, none, True))
+        for pair, (out, running) in zip(held, attend(streams)):
+            acc_own[:, pair_cols(pair)] = out
+            run_own[:, run_cols(pair)] = running
+        return carry
+
+    def near_group(step, carry):
+        held = [pairs - 1 - step * group - index for index in range(group)]
+        for pair in held:
+            for pending in (me == 3, jnp.logical_and(me == 1, pair < len(pairs_of(0)))):
+
+                @pl.when(pending)
+                def _(pair=pair):
+                    for kind in range(2):
+                        arrive(kind, 0, pair)
+
+        streams = []
+        for pair in held:
+            cols = pair_cols(pair)
+            blocks = [
+                (
+                    k_far[0, chunk * LANES : (chunk + 1) * LANES, cols],
+                    v_far[0, chunk * LANES : (chunk + 1) * LANES, cols],
+                    bias_far[0, chunk, pl.ds(pair, 1), :],
+                    0,
+                )
+                for chunk in reversed(range(chunks))
+            ]
+            streams.append((q_norm[:, cols], blocks, run_own[:, run_cols(pair)], False))
+        for pair, (out, running) in zip(held, attend(streams)):
+            acc_own[:, pair_cols(pair)] += out
+            run_own[:, run_cols(pair)] = running
+        return carry
+
+    def far_copy(slot, pair):
+        return pltpu.make_async_remote_copy(
+            src_ref=far_stage.at[slot, :, pair_cols(pair)],
+            dst_ref=far_land.at[:, pair_cols(pair)],
+            send_sem=back_send.at[slot, pair],
+            recv_sem=back_recv.at[pair],
+            device_id={"sp": slot + 2},
+            device_id_type=pl.DeviceIdType.MESH,
+        )
+
+    def far_pair(step, carry):
+        pair = last_pair - 1 - step
+        cols = pair_cols(pair)
+        for owner, due in enumerate(
+            (
+                ((2, 0), (2, 1), (0, 1), (1, 1)),
+                ((2, 0), (2, 1), (0, 0), (1, 0)),
+                ((2, 1), (0, 1), (1, 1), (0, 0), (1, 0)),
             )
-            copy.start()
-            sends.append(copy)
-        source, target = piece(kind, me)
-        copy = pltpu.make_async_copy(source, target, local_sem.at[kind])
-        copy.start()
-        local.append(copy)
-
-    redistribute(3)
-    project(0, mate_rows)
-    redistribute(0)
-    project(3, mate_rows)
+        ):
+
+            @pl.when(me == owner)
+            def _(due=due):
+                for kind, slot in due:
+                    arrive(kind, slot, pair)
+
+        queries = q_far[:, :, cols].reshape(2 * rows, LANES)
+        acc_far[...] = jnp.zeros_like(acc_far)
+        run_far[...] = jnp.zeros_like(run_far)
+
+        def key_block(step, inner):
+            slot = 1 - step
+            blocks = [
+                (
+                    k_far[slot, chunk * LANES : (chunk + 1) * LANES, cols],
+                    v_far[slot, chunk * LANES : (chunk + 1) * LANES, cols],
+                    bias_far[slot, chunk, pl.ds(pair, 1), :],
+                    0,
+                )
+                for chunk in reversed(range(chunks))
+            ]
+            ((out, running),) = attend([(queries, blocks, run_far[...], False)])
+            acc_far[...] += out
+            run_far[...] = running
+            return inner
+
+        lax.fori_loop(0, 2, key_block, 0)
+        for slot in range(2):
+            part = acc_far[slot * rows : (slot + 1) * rows, :].astype(jnp.bfloat16)
+
+            @pl.when(me == slot + 2)
+            def _(part=part):
+                far_land[:, cols] = part
+
+            @pl.when(me != slot + 2)
+            def _(part=part, slot=slot):
+                far_stage[slot, :, cols] = part
+                far_copy(slot, pair).start()
+
+        return carry
+
+    far_count, last_pair = jnp.int32(0), jnp.int32(0)
+    for owner in range(3):
+        if pairs_of(owner):
+            far_count = jnp.where(me == owner, len(pairs_of(owner)), far_count)
+            last_pair = jnp.where(me == owner, pairs_of(owner)[0] + 1, last_pair)
+
+    lax.fori_loop(0, pairs // group, own_group, 0)
+    for owner, (slot, held) in enumerate(
+        (
+            (0, ((k_norm, k_far), (v_ref, v_far), (bias_stage, bias_far))),
+            (1, ((k_norm, k_far), (v_ref, v_far), (bias_stage, bias_far))),
+            (0, ((q_norm, q_far),)),
+        )
+    ):
+
+        @pl.when(me == owner)
+        def _(slot=slot, held=held):
+            for source, target in held:
+                target[slot] = source[...]
+
+    for pair in pairs_of(2):
+        relayed = [(kind, 2, 0, pair, part, True) for part in range(2) for kind in range(2)]
+        sent[1] += relayed
+
+        @pl.when(me == 1)
+        def _(relayed=relayed, pair=pair):
+            for kind in range(2):
+                arrive(kind, 0, pair)
+            for entry in relayed:
+                piece_copy(*entry).start()
+
+    for goal in range(ranks):
+        for index, (_, target, _) in enumerate(BIASES):
+            if target == goal:
+
+                @pl.when(me == goal)
+                def _(index=index):
+                    bias_copy(index).wait_recv()
+
+    far_first = 0
+    weights[3].wait()
+    project(3, whole)
 
     def place(axis):
         index = lax.broadcasted_iota(jnp.int32, (rows, rows), axis)
@@ -514,12 +863,12 @@
     )
     spread_state = jnp.where(spread_state, 1.0, 0.0).astype(jnp.bfloat16)
 
-    def by_channel(ref):
-        wide = jnp.broadcast_to(ref[...][:, None, :], (groups, GROUP, STATE))
+    def by_channel(row):
+        wide = jnp.broadcast_to(plan_ref[row][:, None, :], (groups, GROUP, STATE))
         return wide.reshape(groups * GROUP, STATE)
 
-    factor_r = by_channel(factor_r_ref)
-    factor_i = by_channel(factor_i_ref)
+    factor_r = by_channel(2)
+    factor_i = by_channel(3)
     drive_r = factor_r * input_r_ref[...] - factor_i * input_i_ref[...]
     drive_i = factor_r * input_i_ref[...] + factor_i * input_r_ref[...]
 
@@ -588,10 +937,8 @@
         copy.start()
         end_copies.append(copy)
 
-    project(1, mate_rows)
-    redistribute(1)
-    project(2, mate_rows)
-    redistribute(2)
+    send_late((0, 2), 2)
+    lax.fori_loop(far_first, far_count, far_pair, 0)
 
     for copy in end_copies:
         copy.wait_recv()
@@ -643,85 +990,31 @@
 
     lax.fori_loop(0, pieces, state_piece, 0)
 
-    for copy in local:
-        copy.wait()
-    for copy in sends:
-        copy.wait_recv()
-
-    tail = lax.broadcasted_iota(jnp.int32, (LANES, 2 * LANES), 0)
-    col = lax.broadcasted_iota(jnp.int32, (LANES, 2 * LANES), 1)
-    tail = jnp.where(jnp.logical_or(tail >= col, col >= LANES), 1.0, 0.0).astype(jnp.bfloat16)
-    lane = lax.broadcasted_iota(jnp.int32, (1, LANES), 1)
-    low_mask = jnp.where(lane < HEAD_DIM, 1.0, 0.0).astype(jnp.bfloat16)
-    high_mask = jnp.where(lane < HEAD_DIM, 0.0, 1.0).astype(jnp.bfloat16)
-
-    def chunk_step(chunk, first, diagonal):
-        count = rows - first
-        at = pl.ds(pl.multiple_of(chunk * LANES, LANES), LANES)
-        keys = k_land[at, :]
-        values = v_land[at, :]
-        values = jnp.concatenate([values * low_mask, values * high_mask], axis=0)
-        probs = []
-        for head in range(2):
-            span_rows = slice(head * rows + first, (head + 1) * rows)
-            z = dot_nt(q_two[span_rows, :], keys) + bias_land[chunk, head : head + 1, :]
-            keep = jnp.minimum(-z, 0.0) - jnp.log(1.0 + jnp.exp(-jnp.abs(z)))
-            if diagonal:
-                causal = lax.broadcasted_iota(
-                    jnp.int32, (count, LANES), 1
-                ) < lax.broadcasted_iota(jnp.int32, (count, LANES), 0)
-                keep = jnp.where(causal, keep, 0.0)
-            sums = dot_nn(keep.astype(jnp.bfloat16), tail)
-            running = run_ref[span_rows, :]
-            weight = jnp.exp(z + sums[:, :LANES] + running)
-            if diagonal:
-                weight = jnp.where(causal, weight, 0.0)
-            run_ref[span_rows, :] = running + sums[:, LANES:]
-            probs.append(weight.astype(jnp.bfloat16))
-        acc_ref[first:, :] += dot_nn(jnp.concatenate(probs, axis=1), values)
-
-    def back_copy(step):
-        rank = at_rank(step)
-        return pltpu.make_async_remote_copy(
-            src_ref=out_stage.at[rank],
-            dst_ref=out_land.at[me],
-            send_sem=back_send.at[step],
-            recv_sem=back_recv.at[step],
-            device_id={"sp": rank},
-            device_id_type=pl.DeviceIdType.MESH,
-        )
-
-    def query_block(step, carry):
-        rank = at_rank(step)
-        queries = q_land[pl.ds(pl.multiple_of(rank * rows, rows), rows), :]
-        q_two[:rows, :] = queries * low_mask
-        q_two[rows:, :] = queries * high_mask
-        acc_ref[...] = jnp.zeros_like(acc_ref)
-        run_ref[...] = jnp.zeros_like(run_ref)
-        for part in reversed(range(chunks)):
-            chunk_step(rank * chunks + part, part * LANES, True)
-
-        def earlier(index, inner):
-            for part in reversed(range(chunks)):
-                chunk_step((rank - 1 - index) * chunks + part, 0, False)
-            return inner
-
-        lax.fori_loop(0, rank, earlier, 0)
-        out_stage[rank] = head_rms(acc_ref[...]).astype(jnp.bfloat16)
-
-        @pl.when(step < ranks)
-        def _():
-            back_copy(step).start()
-
-        return carry
-
-    lax.fori_loop(1, ranks + 1, query_block, 0)
-
-    out_land[me] = out_stage[me]
-    for step in others:
-        back_copy(step).wait_recv()
-    for rank in range(ranks):
-        act_ref[:, width + rank * LANES : width + (rank + 1) * LANES] = out_land[rank]
+    @pl.when(lax.rem(me, 2) == 1)
+    def _():
+        lax.fori_loop(0, pairs // group, near_group, 0)
+
+
+    for pair in range(pairs):
+        cols = slice(pair * LANES, (pair + 1) * LANES)
+        for goal in range(2, ranks):
+            if OWNERS[pair] != goal:
+
+                @pl.when(me == goal)
+                def _(pair=pair):
+                    far_copy(0, pair).wait_recv()
+
+        @pl.when(me >= 2)
+        def _(pair=pair, cols=cols):
+            low = run_own[:, 2 * pair * LANES : (2 * pair + 1) * LANES]
+            high = run_own[:, (2 * pair + 1) * LANES : (2 * pair + 2) * LANES]
+            factor = jnp.exp2(-by_head(low, high, low.shape))
+            acc_own[:, cols] += factor * far_land[:, cols].astype(jnp.float32)
+
+        act_ref[:, width + pair * LANES : width + (pair + 1) * LANES] = head_rms(
+            acc_own[:, cols]
+        ).astype(jnp.bfloat16)
+
     def part_copy(index):
         return pltpu.make_async_remote_copy(
             src_ref=out_part.at[index],
@@ -752,10 +1045,22 @@
     row_copy.wait_send()
     for index in range(pieces):
         part_copy(index).wait_send()
-    for copy in sends + end_copies:
+    for copy in end_copies:
         copy.wait_send()
-    for step in others:
-        back_copy(step).wait_send()
+    for origin in range(ranks):
+
+        @pl.when(me == origin)
+        def _(entries=sent[origin]):
+            for entry in entries:
+                (piece_copy if len(entry) > 1 else bias_copy)(*entry).wait_send()
+
+    for pair in range(pairs):
+        for slot in range(2):
+            if OWNERS[pair] != slot + 2:
+
+                @pl.when(me == OWNERS[pair])
+                def _(pair=pair, slot=slot):
+                    far_copy(slot, pair).wait_send()
 
 
 def layer(ranks, tokens, norm_gain, weights, gains, key_bias, plan):
@@ -764,6 +1069,7 @@
     rows = key_bias.shape[0]
     states = plan[0].size
     chunks = rows // LANES
+    pairs = width // LANES
     pieces = features // 512
     bias = key_bias.T
     gains = [gain[None, :] for gain in gains]
@@ -777,6 +1083,7 @@
         in_specs=[vmem] * 2 + [hbm] * 6 + [vmem] * (3 + len(plan)),
         out_specs=vmem,
         scratch_shapes=[
+            pltpu.VMEM((4, *plan[0].shape), full),
             pltpu.VMEM((rows, features), half),
             pltpu.VMEM((2, states), full),
             pltpu.VMEM((rows, features), full),
@@ -787,35 +1094,37 @@
             pltpu.VMEM((rows, width), half),
             pltpu.VMEM((rows, width), half),
             pltpu.VMEM((rows, width), half),
-            pltpu.VMEM((ranks, chunks, 2, LANES), full),
+            pltpu.VMEM((chunks, pairs, 2 * LANES), full),
             pltpu.VMEM((pieces, count, 512), half),
             pltpu.VMEM((pieces, count, 512), half),
             dma((6,)),
             dma((2,)),
             dma((pieces,)),
             dma((pieces,)),
-            pltpu.VMEM((ranks * rows, LANES), half),
-            pltpu.VMEM((ranks * rows, LANES), half),
-            pltpu.VMEM((ranks * rows, LANES), half),
-            pltpu.VMEM((ranks * chunks, 2, LANES), full),
+            pltpu.VMEM((2, rows, width), half),
+            pltpu.VMEM((2, rows, width), half),
+            pltpu.VMEM((2, rows, width), half),
+            pltpu.VMEM((2, chunks, pairs, 2 * LANES), full),
             pltpu.VMEM((rows, states), full),
             pltpu.VMEM((rows, states), full),
             pltpu.VMEM((rows, width), half),
             pltpu.VMEM((8, states), full),
             pltpu.VMEM((8, states), full),
             pltpu.VMEM((ranks, 2, states), full),
-            pltpu.VMEM((2 * rows, LANES), half),
-            pltpu.VMEM((rows, LANES), full),
+            pltpu.VMEM((rows, width), full),
+            pltpu.VMEM((rows, 2 * width), full),
             pltpu.VMEM((2 * rows, LANES), full),
-            pltpu.VMEM((ranks, rows, LANES), half),
-            pltpu.VMEM((ranks, rows, LANES), half),
-            dma((4,)),
-            dma((ranks, 4)),
-            dma((ranks, 4)),
+            pltpu.VMEM((2 * rows, 2 * LANES), full),
+            pltpu.VMEM((2, rows, width), half),
+            pltpu.VMEM((rows, width), half),
+            dma((3, 2, pairs, 2)),
+            dma((3, 2, pairs, 2)),
+            dma((len(BIASES),)),
+            dma((2,)),
             dma((ranks,)),
             dma((ranks,)),
-            dma((ranks + 1,)),
-            dma((ranks + 1,)),
+            dma((2, pairs)),
+            dma((pairs,)),
         ],
         compiler_params=pltpu.CompilerParams(
             collective_id=0, has_side_effects=True, vmem_limit_bytes=58 * 2**20
@@ -849,7 +1158,7 @@
     width = w_query.shape[1]
     rows = key_bias.shape[0]
     fits = (
-        ranks > 1
+        ranks == len(OWNERS)
         and width == ranks * LANES
         and w_input.shape[1] == width
         and width % 256 == 0
@@ -879,15 +1188,10 @@
             w_out_state,
             w_out_attn,
         )
-    ones = jnp.ones_like(eigen_real)[..., None]
-    decay_r, decay_i, factor_r, factor_i = discretize(
-        eigen_real, eigen_imag, log_step, ones, jnp.zeros_like(ones)
-    )
     plan = (
-        decay_r,
-        decay_i,
-        factor_r[..., 0],
-        factor_i[..., 0],
+        eigen_real,
+        eigen_imag,
+        log_step[None, :],
         jnp.transpose(input_real, (0, 2, 1)).reshape(-1, STATE),
         jnp.transpose(input_imag, (0, 2, 1)).reshape(-1, STATE),
         read_real.reshape(-1, STATE),

time: 61.3 us -> 43.4 us (0.71)
  the two profiles are of different devices: /device:TPU:0 before, /device:TPU:11 now
where the time goes in v2:
time: 43.4 us; the launch traced here: 43.2 us
  Pallas kernels  41.1 us (95%)
  local copies, waits for them, and re-layouts  2.09 us (5%)
    pallas_call x1, Pallas kernels, layer(): pl.pallas_call(functools.partial(mixer_kernel, ranks), out_shape=jax.Shap...  41.1 us
    unnamed x1, local copies, waits for them, and re-layouts  2.09 us

profile of v2, /device:TPU:11, one launch (start us, length us, event | category | flops | bytes accessed | tf_op | source)
XLA Modules:
  0.0 43.2 jit_solution(12275079136066914024)
XLA Ops:
  0.0 41.1 %layer.1 = bf16[192,2048]{1,0:T(8,128)(2,1)} custom-call(bf16[192,2048]{1,0:T(8,128)(2,1)} %tokens_ref.1, f32[1,2048]{1,0:T(1,128)} %bitcast.18, bf16[2048,512]{1,0:T(8,128)(2,1)} %w_input_ref.1, bf16[2048,512]{1,0:T(8,128)(2,1)} %w_query_ref.1, bf16[2048,512]{1,0:T(8,128)(2,1)} %w_key_ref.1, bf16[2048,512]{1,0:T(8,128)(2,1)} %w_value_ref.1, ...), custom_call_target="tpu_custom_call" | custom-call | tf_op jit(solution)/shard_map/layer/pallas_call | solution.py:1080
  41.1 2.1 %copy.21 = bf16[192,2048]{1,0:T(8,128)(2,1)} copy(bf16[192,2048]{1,0:T(8,128)(2,1)} %layer.1) | data formatting | bytes 1572864

commit v3 on v2

--- a/solution.py
+++ b/solution.py
@@ -329,7 +329,8 @@
     return [pair for pair, rank in reversed(list(enumerate(OWNERS))) if rank == owner]
 
 
-LATE = 2
+LAST_MERGED = min(pairs_of(1) or [0])
+MERGED = [pair for pair in range(len(OWNERS)) if pair != LAST_MERGED] + [LAST_MERGED]
 
 
 def routes(kind, origin, late=0):
@@ -337,7 +338,7 @@
     if late == 1:
         plan = {0: [(1, 0, pairs_of(1))]}
     elif late == 2:
-        plan = {0: [(1, 0, pairs_of(0))], 2: [(3, 0, every[LATE:])]}
+        plan = {0: [(1, 0, pairs_of(0))]}
     elif kind == "q":
         plan = {
             2: [(0, 0, pairs_of(0)), (1, 0, pairs_of(1))],
@@ -347,7 +348,7 @@
         plan = {
             0: [(1, 0, pairs_of(2))],
             1: [(2, 1, pairs_of(2)), (0, 1, pairs_of(0))],
-            2: [(3, 0, every[:LATE])],
+            2: [(3, 0, [pair for pair in every if OWNERS[pair] != 2])],
         }
     return [(goal, slot, pair) for goal, slot, held in plan.get(origin, []) for pair in held]
 
@@ -476,9 +477,16 @@
     weights = []
     for slot, ref in enumerate((w_key_ref, w_value_ref, w_query_ref, w_input_ref)):
         weights.append(pltpu.make_async_copy(ref, w_held.at[slot], w_sem.at[slot]))
-    for slot, ref in enumerate((w_state_ref, w_attn_ref)):
-        target = w_out.at[slot * width : (slot + 1) * width, :]
-        weights.append(pltpu.make_async_copy(ref, target, w_sem.at[4 + slot]))
+    weights.append(pltpu.make_async_copy(w_state_ref, w_out.at[:width, :], w_sem.at[4]))
+    for place_of, pair in enumerate(MERGED):
+        first = width + place_of * LANES
+        weights.append(
+            pltpu.make_async_copy(
+                w_attn_ref.at[pair * LANES : (pair + 1) * LANES, :],
+                w_out.at[first : first + LANES, :],
+                w_sem.at[5 + place_of],
+            )
+        )
     for low, order in ((True, (0, 1, 2)), (False, (2, 0, 1))):
 
         @pl.when((me < 2) if low else (me >= 2))
@@ -550,8 +558,14 @@
     def send_pieces(kind, part, ranks_of):
         for origin in ranks_of:
             chosen = routes(KINDS[kind], origin)
-            if chosen:
-                send_entries([(kind, *route, part) for route in chosen], origin)
+            leading = [route for route in chosen if route[0] == 0 or kind < 2]
+            entries = [(kind, *route, part) for route in leading]
+            if part == 1:
+                entries += [
+                    (kind, *route, at) for route in chosen if route not in leading for at in range(2)
+                ]
+            if entries:
+                send_entries(entries, origin)
 
     def send_late(ranks_of, late):
         for origin in ranks_of:
@@ -718,7 +732,7 @@
         return carry
 
     def near_group(step, carry):
-        held = [pairs - 1 - step * group - index for index in range(group)]
+        held = [pairs - 1 - step]
         for pair in held:
             for pending in (me == 3, jnp.logical_and(me == 1, pair < len(pairs_of(0)))):
 
@@ -758,11 +772,30 @@
     def far_pair(step, carry):
         pair = last_pair - 1 - step
         cols = pair_cols(pair)
+        acc_far[...] = jnp.zeros_like(acc_far)
+        run_far[...] = jnp.zeros_like(run_far)
+
+        @pl.when(me == 2)
+        def _():
+            arrive(2, 1, pair)
+            blocks = [
+                (
+                    k_norm[chunk * LANES : (chunk + 1) * LANES, cols],
+                    v_ref[chunk * LANES : (chunk + 1) * LANES, cols],
+                    bias_stage[chunk, pl.ds(pair, 1), :],
+                    0,
+                )
+                for chunk in reversed(range(chunks))
+            ]
+            ((out, running),) = attend([(q_far[1, :, cols], blocks, run_far[rows:, :], False)])
+            acc_far[rows:, :] = out
+            run_far[rows:, :] = running
+
         for owner, due in enumerate(
             (
                 ((2, 0), (2, 1), (0, 1), (1, 1)),
                 ((2, 0), (2, 1), (0, 0), (1, 0)),
-                ((2, 1), (0, 1), (1, 1), (0, 0), (1, 0)),
+                ((0, 1), (1, 1), (0, 0), (1, 0)),
             )
         ):
 
@@ -772,9 +805,6 @@
                     arrive(kind, slot, pair)
 
         queries = q_far[:, :, cols].reshape(2 * rows, LANES)
-        acc_far[...] = jnp.zeros_like(acc_far)
-        run_far[...] = jnp.zeros_like(run_far)
-
         def key_block(step, inner):
             slot = 1 - step
             blocks = [
@@ -826,6 +856,26 @@
             for source, target in held:
                 target[slot] = source[...]
 
+    for goal in range(ranks):
+        for index, (_, target, _) in enumerate(BIASES):
+            if target == goal:
+
+                @pl.when(me == goal)
+                def _(index=index):
+                    bias_copy(index).wait_recv()
+
+    weights[3].wait()
+    project(3, whole)
+
+    def place(axis):
+        index = lax.broadcasted_iota(jnp.int32, (rows, rows), axis)
+        other = lax.broadcasted_iota(jnp.int32, (rows, rows), 1 - axis)
+        return jnp.where(other == (index & 7) * seg_len + (index >> 3), 1.0, 0.0).astype(
+            jnp.bfloat16
+        )
+
+    up_ref[...] = dot_nn(place(0), u_ref[...]).astype(jnp.bfloat16)
+
     for pair in pairs_of(2):
         relayed = [(kind, 2, 0, pair, part, True) for part in range(2) for kind in range(2)]
         sent[1] += relayed
@@ -837,26 +887,6 @@
             for entry in relayed:
                 piece_copy(*entry).start()
 
-    for goal in range(ranks):
-        for index, (_, target, _) in enumerate(BIASES):
-            if target == goal:
-
-                @pl.when(me == goal)
-                def _(index=index):
-                    bias_copy(index).wait_recv()
-
-    far_first = 0
-    weights[3].wait()
-    project(3, whole)
-
-    def place(axis):
-        index = lax.broadcasted_iota(jnp.int32, (rows, rows), axis)
-        other = lax.broadcasted_iota(jnp.int32, (rows, rows), 1 - axis)
-        return jnp.where(other == (index & 7) * seg_len + (index >> 3), 1.0, 0.0).astype(
-            jnp.bfloat16
-        )
-
-    up_ref[...] = dot_nn(place(0), u_ref[...]).astype(jnp.bfloat16)
 
     spread_state = lax.broadcasted_iota(jnp.int32, (STATE, span), 0) == (
         lax.broadcasted_iota(jnp.int32, (STATE, span), 1) & (STATE - 1)
@@ -937,8 +967,16 @@
         copy.start()
         end_copies.append(copy)
 
-    send_late((0, 2), 2)
-    lax.fori_loop(far_first, far_count, far_pair, 0)
+    send_late((0,), 2)
+    far_middle = jnp.where(me == 1, jnp.minimum(far_count, 1), far_count)
+    near_first = jnp.where(me == 3, len(pairs_of(2)), 0)
+    near_count = jnp.where(lax.rem(me, 2) == 1, pairs, 0)
+    near_middle = jnp.where(me == 1, len(pairs_of(2)) + 1, near_count)
+    near_start = jnp.where(me == 1, len(pairs_of(2)), near_count)
+    lax.fori_loop(near_first, near_start, near_group, 0)
+    lax.fori_loop(0, far_middle, far_pair, 0)
+    lax.fori_loop(near_start, near_middle, near_group, 0)
+    lax.fori_loop(far_middle, far_count, far_pair, 0)
 
     for copy in end_copies:
         copy.wait_recv()
@@ -974,6 +1012,7 @@
             jnp.bfloat16
         )
 
+    lax.fori_loop(near_middle, near_count, near_group, 0)
     for copy in weights[4:]:
         copy.wait()
     pieces = out_part.shape[0]
@@ -982,38 +1021,37 @@
     def piece_cols(index):
         return pl.ds(pl.multiple_of(index * piece_width, piece_width), piece_width)
 
+    most = 2 * width - LANES
+
     def state_piece(index, carry):
         state_part[:, piece_cols(index)] = dot_nn(
-            act_ref[:, :width], w_out[:width, piece_cols(index)]
+            act_ref[:, :most], w_out[:most, piece_cols(index)]
         )
         return carry
 
-    lax.fori_loop(0, pieces, state_piece, 0)
-
-    @pl.when(lax.rem(me, 2) == 1)
-    def _():
-        lax.fori_loop(0, pairs // group, near_group, 0)
-
-
-    for pair in range(pairs):
+    def merge_pair(place_of, pair):
         cols = slice(pair * LANES, (pair + 1) * LANES)
         for goal in range(2, ranks):
             if OWNERS[pair] != goal:
 
                 @pl.when(me == goal)
-                def _(pair=pair):
+                def _():
                     far_copy(0, pair).wait_recv()
 
         @pl.when(me >= 2)
-        def _(pair=pair, cols=cols):
+        def _():
             low = run_own[:, 2 * pair * LANES : (2 * pair + 1) * LANES]
             high = run_own[:, (2 * pair + 1) * LANES : (2 * pair + 2) * LANES]
             factor = jnp.exp2(-by_head(low, high, low.shape))
             acc_own[:, cols] += factor * far_land[:, cols].astype(jnp.float32)
 
-        act_ref[:, width + pair * LANES : width + (pair + 1) * LANES] = head_rms(
-            acc_own[:, cols]
-        ).astype(jnp.bfloat16)
+        first = width + place_of * LANES
+        act_ref[:, first : first + LANES] = head_rms(acc_own[:, cols]).astype(jnp.bfloat16)
+
+    for place_of, pair in enumerate(MERGED[:-1]):
+        merge_pair(place_of, pair)
+    lax.fori_loop(0, pieces, state_piece, 0)
+    merge_pair(pairs - 1, MERGED[-1])
 
     def part_copy(index):
         return pltpu.make_async_remote_copy(
@@ -1026,7 +1064,7 @@
 
     def piece_of(index, at):
         cols = piece_cols(index)
-        return cols, state_part[at, cols] + dot_nn(act_ref[at, width:], w_out[width:, cols])
+        return cols, state_part[at, cols] + dot_nn(act_ref[at, most:], w_out[most:, cols])
 
     def send_piece(index, carry):
         out_part[index] = piece_of(index, mate_rows)[1].astype(jnp.bfloat16)
@@ -1097,7 +1135,7 @@
             pltpu.VMEM((chunks, pairs, 2 * LANES), full),
             pltpu.VMEM((pieces, count, 512), half),
             pltpu.VMEM((pieces, count, 512), half),
-            dma((6,)),
+            dma((5 + pairs,)),
             dma((2,)),
             dma((pieces,)),
             dma((pieces,)),

time: 43.4 us -> 41.9 us (0.965)
  Pallas kernels: 41.1 us -> 39.6 us
    pallas_call x1, Pallas kernels: 41.1 us -> 39.6 us  [layer(): pl.pallas_call(functools.partial(mixer_kernel, ranks), out_shape=jax.Shap...]
where the time goes in v3:
time: 41.9 us; the launch traced here: 41.7 us
  Pallas kernels  39.6 us (95%)
  local copies, waits for them, and re-layouts  2.09 us (5%)
    pallas_call x1, Pallas kernels, layer(): pl.pallas_call(functools.partial(mixer_kernel, ranks), out_shape=jax.Shap...  39.6 us
    unnamed x1, local copies, waits for them, and re-layouts  2.09 us

profile of v3, /device:TPU:11, one launch (start us, length us, event | category | flops | bytes accessed | tf_op | source)
XLA Modules:
  0.0 41.7 jit_solution(13423715339587418447)
XLA Ops:
  0.0 39.6 %layer.1 = bf16[192,2048]{1,0:T(8,128)(2,1)} custom-call(bf16[192,2048]{1,0:T(8,128)(2,1)} %tokens_ref.1, f32[1,2048]{1,0:T(1,128)} %bitcast.18, bf16[2048,512]{1,0:T(8,128)(2,1)} %w_input_ref.1, bf16[2048,512]{1,0:T(8,128)(2,1)} %w_query_ref.1, bf16[2048,512]{1,0:T(8,128)(2,1)} %w_key_ref.1, bf16[2048,512]{1,0:T(8,128)(2,1)} %w_value_ref.1, ...), custom_call_target="tpu_custom_call" | custom-call | tf_op jit(solution)/shard_map/layer/pallas_call | solution.py:1118
  39.6 2.1 %copy.21 = bf16[192,2048]{1,0:T(8,128)(2,1)} copy(bf16[192,2048]{1,0:T(8,128)(2,1)} %layer.1) | data formatting | bytes 1572864
